TPU v7x, 32 devices: a whole 2x2x4 slice. The times are simulated.
32 devices in a mesh: grp: 2 (over y), ep: 4 (over z), tp: 4 (over x, core).
Axes of the slice: x: 2, y: 2, z: 4, core: 2. Of those that a mesh axis runs over, the one named last changes fastest.
Arguments:
- queries: bfloat16 [4096, 768], P(('grp', 'ep'), 'tp'), parts along dimension 0, may hold values from -6 to 6
- key_value: bfloat16 [4096, 4, 128], P(('grp', 'ep'), 'tp'), parts along dimension 0, may hold values from -6 to 6
- key_bias: bfloat16 [4, 4096], P('tp', ('grp', 'ep')), parts along dimension 1, may hold values from -20 to 0
- out_weight: bfloat16 [768, 2048], P('tp'), may hold values from -0.75 to 0.75
- expert_input: bfloat16 [4096, 2048], P(('grp', 'ep', 'tp')), parts along dimension 0, may hold values from -6 to 6
- norm_gain: float32 [2048], replicated, may hold values from 0.1 to 1.9
- routes: int32 [4096, 4], P(('grp', 'ep', 'tp')), parts along dimension 0, may hold values from 0 to 15, as said below
- route_weights: float32 [4096, 4], P(('grp', 'ep', 'tp')), parts along dimension 0, may hold values from 0.2 to 1
- gate_weight: bfloat16 [16, 2048, 512], P(('ep', 'tp')), may hold values from -0.125 to 0.125
- up_weight: bfloat16 [16, 2048, 512], P(('ep', 'tp')), may hold values from -0.125 to 0.125
- down_weight: bfloat16 [16, 512, 2048], P(('ep', 'tp')), may hold values from -0.25 to 0.25
- shared_gate: bfloat16 [2048, 256], replicated, may hold values from -0.125 to 0.125
- shared_up: bfloat16 [2048, 256], replicated, may hold values from -0.125 to 0.125
- shared_down: bfloat16 [256, 2048], replicated, may hold values from -0.375 to 0.375
Outputs:
- mixer_output: bfloat16 [4096, 2048], P(('grp', 'ep', 'tp')), parts along dimension 0
- expert_output: bfloat16 [4096, 2048], P(('grp', 'ep', 'tp')), parts along dimension 0
There are 2 independent parts, one for each index of `grp`. A program takes and returns all parts, laid end to end along the dimension named above; an argument that names none is the same for every part. Nothing has to cross between parts.
Inputs may be any that keep to these rules, and one draw needn't show every extreme that they name: `routes`: each row names 4 different experts. Among the 128 rows of one device no expert is named more than 48 times, and in every draw one expert is named exactly 48 times in the rows of every device.
All inputs are finite; a program needn't handle non-finite values.
Results may differ from a plain program's by a relative error of at most 0.009.
Values may be sent and summed in bfloat16 or wider, within the bound.
A program may use at most 128 MiB of HBM per device.

v0:
```python
import jax
import jax.numpy as jnp
from jax import lax
from jax.experimental import pallas as pl
from jax.experimental.pallas import tpu as pltpu
from jax.sharding import PartitionSpec as P

MESH = pl.DeviceIdType.MESH
F32 = jnp.float32
BF16 = jnp.bfloat16


def passed_along(block, axis, distance):
    devices = range(lax.axis_size(axis))
    route = [(i - distance, i) for i in devices if i - distance in devices]
    return lax.ppermute(block, axis, route)


def attention_tile(q, k, v, bias, upper, kept, masked):
    z = lax.dot_general(q, k, (((1,), (1,)), ((), ())), preferred_element_type=F32) * 0.125 + bias
    tail = jnp.log(1.0 + jnp.exp(-jnp.abs(z)))
    log_sig = jnp.minimum(z, 0.0) - tail
    keep = -(jnp.maximum(z, 0.0) + tail)
    if masked:
        rows = lax.broadcasted_iota(jnp.int32, z.shape, 0)
        columns = lax.broadcasted_iota(jnp.int32, z.shape, 1)
        allowed = columns < rows
        keep = jnp.where(allowed, keep, 0.0)
    high = keep.astype(BF16)
    low = (keep - high.astype(F32)).astype(BF16)
    after = jnp.dot(high, upper, preferred_element_type=F32)
    after = after + jnp.dot(low, upper, preferred_element_type=F32)
    weight = jnp.exp(log_sig + after + kept)
    if masked:
        weight = jnp.where(allowed, weight, 0.0)
    part = jnp.dot(weight.astype(BF16), v, preferred_element_type=F32)
    return part, kept + jnp.sum(keep, axis=1, keepdims=True)


def attention_kernel(place_ref, q_ref, kv_ref, bias_ref, out_ref, total, kept):
    span, head_dim = q_ref.shape[1:]
    spans = kv_ref.shape[0]
    size = min(span, 256)
    tiles = span // size
    rows = lax.broadcasted_iota(jnp.int32, (size, size), 0)
    columns = lax.broadcasted_iota(jnp.int32, (size, size), 1)
    upper = jnp.where(rows > columns, 1.0, 0.0).astype(BF16)

    def tile(distance, i, j, masked, state):
        there = pl.ds(j * size, size)
        part, after = attention_tile(
            q_ref[0, i * size : (i + 1) * size, :],
            kv_ref[distance, 0, there, :head_dim],
            kv_ref[distance, 0, there, head_dim:],
            bias_ref[distance, 0, :, there].astype(F32),
            upper,
            state[1],
            masked,
        )
        return state[0] + part, after

    for i in range(tiles):
        state = (jnp.zeros((size, head_dim), F32), jnp.zeros((size, 1), F32))
        for j in range(i, -1, -1):
            state = tile(0, i, j, j == i, state)
        total[i] = state[0]
        kept[i] = jnp.broadcast_to(state[1], kept.shape[1:])
    for distance in range(1, spans):

        @pl.when(distance <= place_ref[0])
        def _():
            for i in range(tiles):
                state = (total[i], kept[i, :, :1])
                for j in range(tiles - 1, -1, -1):
                    state = tile(distance, i, j, False, state)
                total[i] = state[0]
                kept[i] = jnp.broadcast_to(state[1], kept.shape[1:])

    for i in range(tiles):
        out_ref[0, i * size : (i + 1) * size, :] = total[i].astype(out_ref.dtype)


def attend(queries, key_value, key_bias):
    span, key_groups, pair_width = key_value.shape
    head_dim = pair_width // 2
    heads = queries.shape[1] // head_dim
    per_group = heads // key_groups
    axis_size = lax.axis_size("ep")
    chain_length = axis_size // max(1, axis_size // 4)
    place = lax.axis_index("ep")
    chain_place = jnp.minimum((place + 2) % chain_length, place)
    furthest = max(min((p + 2) % chain_length, p) for p in range(axis_size))
    packed = jnp.concatenate([key_value.reshape(-1, pair_width), key_bias.reshape(-1, pair_width)])
    visiting = [packed]
    for _ in range(furthest):
        visiting.append(passed_along(visiting[-1], "ep", 1))
    visiting = jnp.stack(visiting)
    keys = visiting[:, : span * key_groups].reshape(-1, span, key_groups, pair_width)
    keys = keys.transpose(0, 2, 1, 3)
    biases = visiting[:, span * key_groups :].reshape(-1, key_groups, 1, span)
    size = min(span, 256)
    attended = pl.pallas_call(
        attention_kernel,
        grid=(heads,),
        out_shape=jax.ShapeDtypeStruct((heads, span, head_dim), BF16),
        in_specs=[
            pl.BlockSpec(memory_space=pltpu.SMEM),
            pl.BlockSpec((1, span, head_dim), lambda h: (h, 0, 0)),
            pl.BlockSpec((furthest + 1, 1, span, pair_width), lambda h: (0, h // per_group, 0, 0)),
            pl.BlockSpec((furthest + 1, 1, 1, span), lambda h: (0, h // per_group, 0, 0)),
        ],
        out_specs=pl.BlockSpec((1, span, head_dim), lambda h: (h, 0, 0)),
        scratch_shapes=[
            pltpu.VMEM((span // size, size, head_dim), F32),
            pltpu.VMEM((span // size, size, 128), F32),
        ],
        name="attention",
        cost_estimate=pl.CostEstimate(flops=4 * 10**9, bytes_accessed=10**6, transcendentals=0),
    )(
        chain_place.reshape(1),
        queries.reshape(span, heads, head_dim).transpose(1, 0, 2),
        keys,
        biases,
    )
    return attended.transpose(1, 0, 2).reshape(span, heads * head_dim)


def project(attended, out_weight):
    return jnp.dot(attended, out_weight, preferred_element_type=F32).astype(BF16)


def exchange_kernel(
    capacity,
    batch,
    terms_ref,
    normed_ref,
    meta_ref,
    shared_gate,
    shared_up,
    shared_down,
    gate_hbm,
    up_hbm,
    down_hbm,
    mixer_ref,
    expert_ref,
    gathered,
    meta,
    gate_v,
    up_v,
    down_v,
    chosen,
    shared,
    sums,
    from_sibling,
    from_side,
    from_line,
    mixer_sibling,
    mixer_side,
    mixer_sum,
    load_sem,
    meta_send,
    meta_recv,
    zs_send,
    zs_recv,
    x_send,
    x_recv,
    s_send,
    s_recv,
    rz_send,
    rz_recv,
    rx_send,
    rx_recv,
    rs_send,
    rs_recv,
    m_send,
    m_recv,
):
    count = lax.axis_size("ep")
    width = normed_ref.shape[1]
    tokens = normed_ref.shape[0]
    cut = width // 8
    spans = (slice(0, cut), slice(cut, width))
    pieces = (pl.ds(0, cut), pl.ds(cut, width - cut))
    z = lax.axis_index("ep")
    t = lax.axis_index("tp")
    x, c = t // 2, t % 2
    ox, oc = 1 - x, 1 - c
    side, sibling = ox * 2 + c, x * 2 + oc
    group = count * 4
    me = z * 4 + t

    loads = [
        pltpu.make_async_copy(a, b, load_sem.at[i])
        for i, (a, b) in enumerate(((gate_hbm, gate_v), (up_hbm, up_v), (down_hbm, down_v)))
    ]
    own_load = pltpu.make_async_copy(normed_ref, gathered.at[z, x, c], load_sem.at[3])
    own_meta = pltpu.make_async_copy(meta_ref.at[me], meta.at[me], load_sem.at[4])
    own_load.start()
    own_meta.start()

    barrier = pltpu.get_barrier_semaphore()
    for step in range(1, group):
        other = (me + step) % group
        pl.semaphore_signal(
            barrier, 1, device_id={"ep": other // 4, "tp": other % 4}, device_id_type=MESH
        )
    pl.semaphore_wait(barrier, group - 1)

    def copy(src, dst, send, recv, ep, tp):
        return pltpu.make_async_remote_copy(
            src_ref=src,
            dst_ref=dst,
            send_sem=send,
            recv_sem=recv,
            device_id={"ep": ep, "tp": tp},
            device_id_type=MESH,
        )

    own_load.wait()
    own_meta.wait()

    def part(zz, xx, cc, h):
        return gathered.at[zz, xx, cc, :, pieces[h]]

    def line(up, kind, zz):
        block = part(zz, ox if kind == 1 else x, c, 1 if kind == 2 else 0)
        return copy(
            block,
            block,
            zs_send.at[0 if up else 1, kind, zz],
            zs_recv.at[kind, zz],
            z + (1 if up else -1),
            t,
        )

    def across(slot, zz):
        block = part(zz, x, c, 0 if slot == 0 else 1)
        index = 0 if slot == 0 else 1 + zz
        return copy(block, block, x_send.at[index], x_recv.at[index], z, side)

    def across_in(slot, zz):
        block = part(zz, ox, c, 0 if slot == 0 else 1)
        index = 0 if slot == 0 else 1 + zz
        return copy(block, block, x_send.at[index], x_recv.at[index], z, side)

    def share(zz, xx, h):
        block = part(zz, xx, c, h)
        return copy(block, block, s_send.at[zz, xx, h], s_recv.at[zz, xx, h], z, sibling)

    def share_in(zz, xx, h):
        block = part(zz, xx, oc, h)
        return copy(block, block, s_send.at[zz, xx, h], s_recv.at[zz, xx, h], z, sibling)

    def meta_copy(step):
        other = (me + step) % group
        return copy(
            meta_ref.at[other],
            meta.at[me],
            meta_send.at[step - 1],
            meta_recv.at[step - 1],
            other // 4,
            other % 4,
        )

    def meta_in(step):
        other = (me + group - step) % group
        return copy(
            meta_ref.at[other],
            meta.at[other],
            meta_send.at[step - 1],
            meta_recv.at[step - 1],
            other // 4,
            other % 4,
        )

    can_up, can_down = z + 1 < count, z >= 1
    slots = lax.broadcasted_iota(jnp.int32, (capacity, tokens), 0).astype(F32)

    def picker(source):
        return jnp.where(meta[source, 1:2, :] == slots, 1.0, 0.0)

    def rows_of(source):
        return pl.ds(pl.multiple_of(source * capacity, 16), capacity)

    def pick(zz, xx, cc, h):
        source = zz * 4 + xx * 2 + cc
        columns = spans[h]
        chosen[rows_of(source), columns] = jnp.dot(
            picker(source).astype(BF16),
            gathered[zz, xx, cc, :, columns],
            preferred_element_type=F32,
        ).astype(BF16)

    def pick_both(zz, xx, h):
        pick(zz, xx, c, h)
        share_in(zz, xx, h).wait_recv()
        pick(zz, xx, oc, h)

    across(0, z).start()
    for kind in (2, 0):

        @pl.when(can_up)
        def _():
            line(True, kind, z).start()

        @pl.when(can_down)
        def _():
            line(False, kind, z).start()

    across(1, z).start()
    for step in range(1, group):
        meta_copy(step).start()
    share(z, x, 0).start()
    share(z, x, 1).start()
    for load in loads:
        load.start()

    def mixer_pair(xx):
        return copy(
            terms_ref.at[xx, oc],
            mixer_sibling.at[xx],
            m_send.at[xx],
            m_recv.at[xx],
            z,
            sibling,
        )

    for xx in range(2):
        mixer_pair(xx).start()

    hidden_gate = jnp.dot(normed_ref[...], shared_gate[...], preferred_element_type=F32)
    hidden_up = jnp.dot(normed_ref[...], shared_up[...], preferred_element_type=F32)
    shared_hidden = (hidden_gate / (1.0 + jnp.exp(-hidden_gate)) * hidden_up).astype(BF16)
    shared[...] = jnp.dot(shared_hidden, shared_down[...], preferred_element_type=F32)

    across_in(0, z).wait_recv()

    @pl.when(can_up)
    def _():
        line(True, 1, z).start()

    @pl.when(can_down)
    def _():
        line(False, 1, z).start()

    share(z, ox, 0).start()
    for step in range(1, group):
        meta_in(step).wait_recv()
    pick_both(z, x, 0)
    pick_both(z, x, 1)
    pick_both(z, ox, 0)

    def other_side(zz):
        across_in(1, zz).wait_recv()
        share(zz, ox, 1).start()
        pick_both(zz, ox, 1)

    for distance in range(1, count):
        below, above = z - distance, z + distance

        def arrive(kind, zz, going_up, further):
            line(going_up, kind, zz).wait_recv()

            @pl.when(further)
            def _():
                line(going_up, kind, zz).start()

            if kind == 2:
                across(1, zz).start()
            share(zz, ox if kind == 1 else x, 1 if kind == 2 else 0).start()

        for kind in (2, 0, 1):

            @pl.when(below >= 0)
            def _():
                arrive(kind, below, True, can_up)

            @pl.when(above < count)
            def _():
                arrive(kind, above, False, can_down)

            for there, zz in ((below >= 0, below), (above < count, above)):

                @pl.when(there)
                def _():
                    pick_both(zz, ox if kind == 1 else x, 1 if kind == 2 else 0)

        for there, zz in (
            ((z >= 0, z),)
            if distance == 1
            else ((below + 1 >= 0, below + 1), (above - 1 < count, above - 1))
        ):

            @pl.when(there)
            def _():
                other_side(zz)

    for xx in range(2):
        mixer_pair(xx).wait()
    mixer_sum[...] = (
        terms_ref[ox, c].astype(F32) + mixer_sibling[ox].astype(F32)
    ).astype(BF16)
    mixer_move = copy(mixer_sum, mixer_side, m_send.at[2], m_recv.at[2], z, side)
    mixer_move.start()

    for zz in (z - (count - 1), z + (count - 1)):

        @pl.when((zz >= 0) & (zz < count))
        def _():
            other_side(zz)

    for load in loads:
        load.wait()

    @pl.loop(0, group // batch)
    def _(turn):
        block = pl.ds(pl.multiple_of(turn * (batch * capacity), 16), batch * capacity)
        scales = []
        for i in range(batch):
            source = turn * batch + i
            scales.append(
                jnp.sum(picker(source) * meta[source, 0:1, :], axis=1, keepdims=True)
            )
        scale = jnp.concatenate(scales, axis=0)
        gate = jnp.dot(chosen[block, :], gate_v[...], preferred_element_type=F32)
        up = jnp.dot(chosen[block, :], up_v[...], preferred_element_type=F32)
        hidden = (gate / (1.0 + jnp.exp(-gate)) * up).astype(BF16)
        rows = jnp.dot(hidden, down_v[...], preferred_element_type=F32)
        chosen[block, :] = (rows * scale).astype(BF16)

    def spread(zz, xx, cc):
        source = zz * 4 + xx * 2 + cc
        sums[zz, xx, cc] = lax.dot_general(
            picker(source).astype(BF16),
            chosen[rows_of(source), :],
            (((0,), (0,)), ((), ())),
            preferred_element_type=F32,
        ).astype(BF16)

    def pair(zz, xx):
        return copy(
            sums.at[zz, xx, oc],
            from_sibling.at[zz, xx],
            rs_send.at[zz, xx],
            rs_recv.at[zz, xx],
            z,
            sibling,
        )

    def half_ref(zz, xx, h):
        return sums.at[zz, xx, c, :, pieces[h]]

    def side_ref(h, zz):
        return from_side.at[1 + zz] if h else from_side.at[0, :, pieces[0]]

    def line_ref(up, kind, zz):
        slot = from_line.at[0 if up else 1, kind, zz]
        return slot if kind == 2 else slot.at[:, pieces[0]]

    def side_move(zz):
        return copy(
            half_ref(zz, ox, 1), side_ref(1, zz), rx_send.at[1 + zz], rx_recv.at[1 + zz], z, side
        )

    def last_move():
        return copy(half_ref(z, ox, 0), side_ref(0, z), rx_send.at[0], rx_recv.at[0], z, side)

    def back(up, kind, zz):
        return copy(
            half_ref(zz, ox if kind == 1 else x, 1 if kind == 2 else 0),
            line_ref(up, kind, zz),
            rz_send.at[kind, zz],
            rz_recv.at[0 if up else 1, kind, zz],
            z + (1 if up else -1),
            t,
        )

    def add(ref, other):
        ref[...] = (ref[...].astype(F32) + other[...].astype(F32)).astype(BF16)

    order = []
    for k in range(count - 1):
        low = (count - 1 - k) - (z - (count - 1 - k) + count) // count
        high = k + (k - z + count) // count
        order.append(low + (z // (count // 2)) * (high - low))
    order.append(z)

    def finish(zz, own):
        for xx in (ox, x):
            pair(zz, xx).wait_recv()
            add(sums.at[zz, xx, c], from_sibling.at[zz, xx])
        side_move(zz).start()
        if not own:
            for up, edge in ((True, z == 0), (False, z == count - 1)):

                @pl.when(edge)
                def _():
                    back(up, 1, zz).start()
                    back(up, 0, zz).start()

    for k in range(count + 1):
        if k < count:
            for xx in (ox, x):
                spread(order[k], xx, oc)
                pair(order[k], xx).start()
            for xx in (ox, x):
                spread(order[k], xx, c)
        if k >= 1:
            finish(order[k - 1], k == count)

    for distance in range(count - 1, 0, -1):
        for kind in (1, 0, 2):
            for up in (True, False):
                target = z + distance if up else z - distance
                exists = target < count if up else target >= 0
                feeds = can_down if up else can_up

                @pl.when(exists)
                def _():
                    mine = half_ref(target, ox if kind == 1 else x, 1 if kind == 2 else 0)
                    if kind == 2:
                        side_move(target).wait_recv()
                        add(mine, from_side.at[1 + target])

                    @pl.when(feeds)
                    def _():
                        back(up, kind, target).wait_recv()
                        add(mine, line_ref(up, kind, target))
                        if kind != 2:
                            back(up, kind, target).start()

                    if kind == 2:
                        back(up, kind, target).start()

    for kind in (1, 0, 2):
        mine = half_ref(z, ox if kind == 1 else x, 1 if kind == 2 else 0)
        if kind == 2:
            side_move(z).wait_recv()
            add(mine, from_side.at[1 + z])
        for up in (True, False):

            @pl.when(can_down if up else can_up)
            def _():
                back(up, kind, z).wait_recv()
                add(mine, line_ref(up, kind, z))

        if kind == 1:
            last_move().start()

    mixer_move.wait()
    mixer_ref[...] = (
        terms_ref[x, c].astype(F32)
        + mixer_sibling[x].astype(F32)
        + mixer_side[...].astype(F32)
    ).astype(BF16)
    expert_ref[:, cut:] = (sums[z, x, c, :, cut:].astype(F32) + shared[:, cut:]).astype(BF16)
    last_move().wait_recv()
    expert_ref[:, :cut] = (
        sums[z, x, c, :, :cut].astype(F32) + from_side[0, :, :cut].astype(F32) + shared[:, :cut]
    ).astype(BF16)

    for step in range(1, group):
        meta_copy(step).wait_send()
    across(0, z).wait_send()
    last_move().wait_send()
    for zz in range(count):
        across(1, zz).wait_send()
        side_move(zz).wait_send()
        for xx in range(2):
            pair(zz, xx).wait_send()
            for h in range(2):
                share(zz, xx, h).wait_send()
        for kind in range(3):

            @pl.when((zz <= z) & can_up)
            def _():
                line(True, kind, zz).wait_send()

            @pl.when((zz >= z) & can_down)
            def _():
                line(False, kind, zz).wait_send()

            @pl.when(zz > z)
            def _():
                back(True, kind, zz).wait_send()

            @pl.when(zz < z)
            def _():
                back(False, kind, zz).wait_send()


def exchange(terms, normed, meta, shared_parts, routed_parts, capacity):
    tokens, width = normed.shape
    count = lax.axis_size("ep")
    group = count * 4
    hidden = routed_parts[0].shape[1]
    rest = width - width // 8
    batch = 8 if group % 8 == 0 else 4
    dma = pltpu.SemaphoreType.DMA
    vmem = pl.BlockSpec(memory_space=pltpu.VMEM)
    return pl.pallas_call(
        lambda *refs: exchange_kernel(capacity, batch, *refs),
        out_shape=[jax.ShapeDtypeStruct((tokens, width), BF16)] * 2,
        in_specs=[vmem] * 6 + [pl.BlockSpec(memory_space=pl.ANY)] * 3,
        out_specs=[vmem] * 2,
        scratch_shapes=[
            pltpu.VMEM((count, 2, 2, tokens, width), BF16),
            pltpu.VMEM(meta.shape, F32),
            pltpu.VMEM((width, hidden), BF16),
            pltpu.VMEM((width, hidden), BF16),
            pltpu.VMEM((hidden, width), BF16),
            pltpu.VMEM((group * capacity, width), BF16),
            pltpu.VMEM((tokens, width), F32),
            pltpu.VMEM((count, 2, 2, tokens, width), BF16),
            pltpu.VMEM((count, 2, tokens, width), BF16),
            pltpu.VMEM((1 + count, tokens, rest), BF16),
            pltpu.VMEM((2, 3, count, tokens, rest), BF16),
            pltpu.VMEM((2, tokens, width), BF16),
            pltpu.VMEM((tokens, width), BF16),
            pltpu.VMEM((tokens, width), BF16),
            dma((5,)),
            dma((group - 1,)),
            dma((group - 1,)),
            dma((2, 3, count)),
            dma((3, count)),
            dma((1 + count,)),
            dma((1 + count,)),
            dma((count, 2, 2)),
            dma((count, 2, 2)),
            dma((3, count)),
            dma((2, 3, count)),
            dma((1 + count,)),
            dma((1 + count,)),
            dma((count, 2)),
            dma((count, 2)),
            dma((3,)),
            dma((3,)),
        ],
        compiler_params=pltpu.CompilerParams(
            collective_id=0, has_side_effects=True, vmem_limit_bytes=60 * 2**20
        ),
        name="exchange",
        cost_estimate=pl.CostEstimate(flops=10**10, bytes_accessed=2 * 10**7, transcendentals=0),
    )(terms.reshape(2, 2, tokens, width), normed, meta, *shared_parts, *routed_parts)


def normalise(expert_input, norm_gain):
    widened = expert_input.astype(F32)
    return (
        widened * lax.rsqrt(jnp.mean(widened * widened, axis=-1, keepdims=True) + 1e-06) * norm_gain
    ).astype(BF16)


def route_table(routes, route_weights, experts):
    tokens = routes.shape[0]
    named = routes[:, None, :] == jnp.arange(experts, dtype=jnp.int32)[None, :, None]
    weight = jnp.sum(jnp.where(named, route_weights[:, None, :], 0.0), axis=2)
    chosen = jnp.any(named, axis=2)
    earlier = jnp.arange(tokens)[None, :] < jnp.arange(tokens)[:, None]
    slot = jnp.dot(earlier.astype(BF16), chosen.astype(BF16), preferred_element_type=F32)
    slot = jnp.where(chosen, slot, -1.0)
    table = jnp.stack([weight.T, slot.T], axis=1)
    return jnp.pad(table, ((0, 0), (0, 6), (0, 0)))


def expert_rows(arrived, gate_weight, up_weight, down_weight):
    sources, capacity, model_width = arrived.shape
    flat_rows = arrived.reshape(sources * capacity, model_width)
    gate_part = jnp.dot(flat_rows, gate_weight[0], preferred_element_type=jnp.float32)
    up_part = jnp.dot(flat_rows, up_weight[0], preferred_element_type=jnp.float32)
    hidden = (jax.nn.silu(gate_part) * up_part).astype(jnp.bfloat16)
    result = jnp.dot(hidden, down_weight[0], preferred_element_type=jnp.float32).astype(
        jnp.bfloat16
    )
    return result.reshape(sources, capacity, model_width)


def experts_half(
    expert_input,
    norm_gain,
    routes,
    route_weights,
    gate_weight,
    up_weight,
    down_weight,
    shared_gate,
    shared_up,
    shared_down,
):
    tokens, top_count = routes.shape
    model_width = expert_input.shape[1]
    ep_count = lax.axis_size("ep")
    tp_count = lax.axis_size("tp")
    experts = ep_count * tp_count
    capacity = max(2, 3 * tokens * top_count // (2 * experts))
    widened = expert_input.astype(jnp.float32)
    normed = (
        widened * lax.rsqrt(jnp.mean(widened * widened, axis=-1, keepdims=True) + 1e-06) * norm_gain
    ).astype(jnp.bfloat16)
    flat_routes = routes.reshape(-1)
    one_hot = (flat_routes[:, None] == jnp.arange(experts, dtype=jnp.int32)[None, :]).astype(
        jnp.int32
    )
    before = jnp.cumsum(one_hot, axis=0) - one_hot
    slot_index = jnp.sum(before * one_hot, axis=1)
    target = flat_routes * capacity + slot_index
    picker = (jnp.arange(experts * capacity, dtype=jnp.int32)[:, None] == target[None, :]).astype(
        jnp.bfloat16
    )
    picker = jnp.sum(picker.reshape(experts * capacity, tokens, top_count), axis=2)
    outgoing = jnp.dot(picker, normed, preferred_element_type=jnp.float32).astype(jnp.bfloat16)
    outgoing = outgoing.reshape(experts, capacity, model_width)
    came_back = lax.all_to_all(
        expert_rows(
            lax.all_to_all(outgoing, ("ep", "tp"), split_axis=0, concat_axis=0, tiled=True),
            gate_weight,
            up_weight,
            down_weight,
        ),
        ("ep", "tp"),
        split_axis=0,
        concat_axis=0,
        tiled=True,
    )
    back_rows = came_back.reshape(experts * capacity, model_width)
    picked = jnp.take(back_rows, target, axis=0).reshape(tokens, top_count, model_width)
    routed = jnp.sum(picked.astype(jnp.float32) * route_weights[:, :, None], axis=1)
    shared_hidden = (
        jax.nn.silu(jnp.dot(normed, shared_gate, preferred_element_type=jnp.float32))
        * jnp.dot(normed, shared_up, preferred_element_type=jnp.float32)
    ).astype(jnp.bfloat16)
    shared_term = jnp.dot(shared_hidden, shared_down, preferred_element_type=jnp.float32)
    return (routed + shared_term).astype(jnp.bfloat16)


def per_device(
    queries,
    key_value,
    key_bias,
    out_weight,
    expert_input,
    norm_gain,
    routes,
    route_weights,
    gate_weight,
    up_weight,
    down_weight,
    shared_gate,
    shared_up,
    shared_down,
):
    terms = project(attend(queries, key_value, key_bias), out_weight)
    tokens, top_count = routes.shape
    width = expert_input.shape[1]
    tp_count = lax.axis_size("tp")
    experts = lax.axis_size("ep") * tp_count
    capacity = max(2, 3 * tokens * top_count // (2 * experts))
    if tp_count == 4 and capacity % 16 == 0 and experts * tokens * width * 2 <= 8 * 2**20:
        mixer_output, expert_output = exchange(
            terms,
            normalise(expert_input, norm_gain),
            route_table(routes, route_weights, experts),
            (shared_gate, shared_up, shared_down),
            (gate_weight[0], up_weight[0], down_weight[0]),
            capacity,
        )
        return (mixer_output, expert_output)
    mixer_output = lax.psum_scatter(terms, "tp", scatter_dimension=0, tiled=True)
    expert_output = experts_half(
        expert_input,
        norm_gain,
        routes,
        route_weights,
        gate_weight,
        up_weight,
        down_weight,
        shared_gate,
        shared_up,
        shared_down,
    )
    return (mixer_output, expert_output)


def solution(mesh):
    placed = (
        P(("grp", "ep"), "tp"),
        P(("grp", "ep"), "tp", None),
        P("tp", ("grp", "ep")),
        P("tp", None),
        P(("grp", "ep", "tp"), None),
        P(),
        P(("grp", "ep", "tp"), None),
        P(("grp", "ep", "tp"), None),
        P(("ep", "tp"), None, None),
        P(("ep", "tp"), None, None),
        P(("ep", "tp"), None, None),
        P(),
        P(),
        P(),
    )
    return jax.shard_map(
        per_device,
        mesh=mesh,
        in_specs=placed,
        out_specs=(P(("grp", "ep", "tp"), None), P(("grp", "ep", "tp"), None)),
        check_vma=False,
    )
```

profile of v0, /device:TPU:0, one launch (start us, length us, event | category | flops | bytes accessed | tf_op | source)
XLA Modules:
  0.0 147.6 jit_solution(12372504665501102360)
XLA Ops:
  0.6 0.0 copy-start
  0.6 0.0 copy-start.1
  0.7 0.8 reduce
  1.4 0.9 pad_maximum_fusion
  2.4 5.0 %collective-permute-start = (bf16[516,128]{1,0:T(8,128)(2,1)S(1)}, bf16[516,128]{1,0:T(8,128)(2,1)S(1)}, u32[]{:S(2)}, u32[]{:S(2)}) collective-permute-start(bf16[516,128]{1,0:T(8,128)(2,1)S(1)} %get-tuple-element.2), channel_id=1, source_target_pairs={{0,4},{4,8},{8,12},{1,5},{5,9},{9,13},{2,6},{6,10},{10,14},{3,7},{... | collective-permute-start | bytes 396296 | tf_op jit(solution)/shard_map/ppermute | solution.py:16
  7.4 1.2 fusion
  8.6 0.7 fusion.5
  9.3 0.1 convolution_select_fusion
  9.4 2.0 %fusion.2.refs_1_ = bf16[128,2048]{1,0:T(8,128)(2,1)} fusion(bf16[128,2048]{1,0:T(8,128)(2,1)} %param.18, f32[2048]{0:T(1024)} %param.19, f32[128]{0:T(128)S(1)} %add_rsqrt_fusion), kind=kLoop, calls=%fused_computation.6 | loop fusion | flops 1048576 | bytes 1057280 | tf_op jit(solution)/shard_map/convert_element_type | solution.py:651
  11.5 0.7 select_reduce_fusion
  12.2 0.0 copy-done.1
  12.2 0.9 copy.23
  13.1 0.6 select_maximum_fusion.refs_2_
  13.8 0.0 collective-permute-done
  13.8 0.7 fusion.4.kv_ref
  14.5 0.6 reshape.43.bias_ref
  15.1 5.6 %attention.1 = bf16[3,512,64]{2,1,0:T(8,128)(2,1)} custom-call(s32[1]{0:T(128)} %bitcast.place_ref, bf16[3,512,64]{2,1,0:T(8,128)(2,1)} %bitcast.29, bf16[2,1,512,128]{3,2,1,0:T(8,128)(2,1)} %fusion.4.kv_ref, bf16[2,1,1,512]{3,2,1,0:T(2,128)(2,1)} %reshape.43.bias_ref), custom_call_target="tpu_custom_call" | custom-call | flops 4000000000 | bytes 1000000 | tf_op jit(solution)/shard_map/attention/pallas_call | solution.py:102
  20.7 1.1 copy.25
  21.8 0.0 copy-done
  21.8 2.1 %convolution_convert_fusion = bf16[512,2048]{1,0:T(8,128)(2,1)} fusion(bf16[512,192]{0,1:T(8,128)(2,1)S(1)} %bitcast.26, bf16[192,2048]{1,0:T(8,128)(2,1)S(1)} %copy-done), kind=kOutput, calls=%fused_computation | convolution fusion | flops 403701760 | bytes 3080192 | tf_op jit(solution)/shard_map/dot_general | solution.py:129
  23.9 119.9 %exchange.1 = (bf16[128,2048]{1,0:T(8,128)(2,1)}, bf16[128,2048]{1,0:T(8,128)(2,1)}) custom-call(bf16[2,2,128,2048]{3,2,1,0:T(8,128)(2,1)} %bitcast.25, bf16[128,2048]{1,0:T(8,128)(2,1)} %fusion.2.refs_1_, f32[16,8,128]{2,1,0:T(8,128)} %select_maximum_fusion.refs_2_, bf16[2048,256]{1,0:T(8,128)(2,1)} %refs_3_.1, bf16[2048,256]{1,0:T(8,128)(2,1)} %refs_4_.1, ...), custom_call_target="tpu_custom_call" | custom-call | flops 10000000000 | bytes 20000000 | tf_op jit(solution)/shard_map/exchange/pallas_call | solution.py:601
  143.8 1.9 %copy.28 = bf16[128,2048]{1,0:T(8,128)(2,1)} copy(bf16[128,2048]{1,0:T(8,128)(2,1)} %get-tuple-element.6) | data formatting | bytes 1048576
  145.7 1.9 %copy.29 = bf16[128,2048]{1,0:T(8,128)(2,1)} copy(bf16[128,2048]{1,0:T(8,128)(2,1)} %get-tuple-element.7) | data formatting | bytes 1048576
  (2 shorter events, 0.0 us)
Async XLA Ops:
  0.6 21.2 %copy-start = (bf16[192,2048]{1,0:T(8,128)(2,1)S(1)}, bf16[192,2048]{1,0:T(8,128)(2,1)}, u32[]{:S(2)}) copy-start(bf16[192,2048]{1,0:T(8,128)(2,1)} %param.17) | copy-start | bytes 2359300
  0.6 11.6 %copy-start.1 = (bf16[512,192]{0,1:T(8,128)(2,1)S(1)}, bf16[512,192]{0,1:T(8,128)(2,1)}, u32[]{:S(2)}) copy-start(bf16[512,192]{0,1:T(8,128)(2,1)} %param.14) | copy-start | bytes 589828
  2.4 11.4 %collective-permute-start = (bf16[516,128]{1,0:T(8,128)(2,1)S(1)}, bf16[516,128]{1,0:T(8,128)(2,1)S(1)}, u32[]{:S(2)}, u32[]{:S(2)}) collective-permute-start(bf16[516,128]{1,0:T(8,128)(2,1)S(1)} %get-tuple-element.2), channel_id=1, source_target_pairs={{0,4},{4,8},{8,12},{1,5},{5,9},{9,13},{2,6},{6,10},{10,14},{3,7},{... | collective-permute-start | bytes 396296 | tf_op jit(solution)/shard_map/ppermute | solution.py:16
where the time goes:
time: 148 us
  Pallas kernels  125 us (84%)
  other arithmetic  7.79 us (5%)
  local copies, waits for them, and re-layouts  6.43 us (4%)
  starting transfers between devices  4.96 us (3%)
  matrix products  2.24 us (2%)
    pallas_call x1, Pallas kernels, exchange(): pl.pallas_call(lambda *refs: exchange_kernel(capacity, batch, *refs), out...  120 us
    pallas_call x1, Pallas kernels, attend(): pl.pallas_call(attention_kernel, grid=(heads,), out_shape=jax.ShapeDtypeS...  5.59 us
    ppermute x1, starting transfers between devices, passed_along(): return lax.ppermute(block, axis, route)  4.96 us
    unnamed x6, local copies, waits for them, and re-layouts  3.78 us
  transfers between devices with their start and end apart: 1, of which 0 were waited for; matrix products, arithmetic and copies ran while one was open for 4% of the time, Pallas kernels for 0%

commit v1 on v0

v1 whole, which is shorter than its diff:
```python
import jax
import jax.numpy as jnp
from jax import lax
from jax.experimental import pallas as pl
from jax.experimental.pallas import tpu as pltpu
from jax.sharding import PartitionSpec as P

MESH = pl.DeviceIdType.MESH
F32 = jnp.float32
BF16 = jnp.bfloat16


def passed_along(block, axis, distance):
    devices = range(lax.axis_size(axis))
    route = [(i - distance, i) for i in devices if i - distance in devices]
    return lax.ppermute(block, axis, route)


def furthest_place(axis_size):
    chain_length = axis_size // max(1, axis_size // 4)
    return max(min((p + 2) % chain_length, p) for p in range(axis_size))


def attention_tile(q, k, v, bias, upper, kept, masked):
    z = lax.dot_general(q, k, (((1,), (1,)), ((), ())), preferred_element_type=F32) * 0.125 + bias
    tail = jnp.log(1.0 + jnp.exp(-jnp.abs(z)))
    log_sig = jnp.minimum(z, 0.0) - tail
    keep = -(jnp.maximum(z, 0.0) + tail)
    if masked:
        rows = lax.broadcasted_iota(jnp.int32, z.shape, 0)
        columns = lax.broadcasted_iota(jnp.int32, z.shape, 1)
        allowed = columns < rows
        keep = jnp.where(allowed, keep, 0.0)
    high = keep.astype(BF16)
    low = (keep - high.astype(F32)).astype(BF16)
    after = jnp.dot(high, upper, preferred_element_type=F32)
    after = after + jnp.dot(low, upper, preferred_element_type=F32)
    weight = jnp.exp(log_sig + after + kept)
    if masked:
        weight = jnp.where(allowed, weight, 0.0)
    part = jnp.dot(weight.astype(BF16), v, preferred_element_type=F32)
    return part, kept + jnp.sum(keep, axis=1, keepdims=True)


def attention_kernel(place_ref, q_ref, kv_ref, bias_ref, out_ref, total, kept):
    span, head_dim = q_ref.shape[1:]
    spans = kv_ref.shape[0]
    size = min(span, 256)
    tiles = span // size
    rows = lax.broadcasted_iota(jnp.int32, (size, size), 0)
    columns = lax.broadcasted_iota(jnp.int32, (size, size), 1)
    upper = jnp.where(rows > columns, 1.0, 0.0).astype(BF16)

    def tile(distance, i, j, masked, state):
        there = pl.ds(j * size, size)
        part, after = attention_tile(
            q_ref[0, i * size : (i + 1) * size, :],
            kv_ref[distance, 0, there, :head_dim],
            kv_ref[distance, 0, there, head_dim:],
            bias_ref[distance, 0, :, there].astype(F32),
            upper,
            state[1],
            masked,
        )
        return state[0] + part, after

    for i in range(tiles):
        state = (jnp.zeros((size, head_dim), F32), jnp.zeros((size, 1), F32))
        for j in range(i, -1, -1):
            state = tile(0, i, j, j == i, state)
        total[i] = state[0]
        kept[i] = jnp.broadcast_to(state[1], kept.shape[1:])
    for distance in range(1, spans):

        @pl.when(distance <= place_ref[0])
        def _():
            for i in range(tiles):
                state = (total[i], kept[i, :, :1])
                for j in range(tiles - 1, -1, -1):
                    state = tile(distance, i, j, False, state)
                total[i] = state[0]
                kept[i] = jnp.broadcast_to(state[1], kept.shape[1:])

    for i in range(tiles):
        out_ref[0, i * size : (i + 1) * size, :] = total[i].astype(out_ref.dtype)


def attend(queries, key_value, key_bias):
    span, key_groups, pair_width = key_value.shape
    head_dim = pair_width // 2
    heads = queries.shape[1] // head_dim
    per_group = heads // key_groups
    axis_size = lax.axis_size("ep")
    chain_length = axis_size // max(1, axis_size // 4)
    place = lax.axis_index("ep")
    chain_place = jnp.minimum((place + 2) % chain_length, place)
    furthest = furthest_place(axis_size)
    packed = jnp.concatenate([key_value.reshape(-1, pair_width), key_bias.reshape(-1, pair_width)])
    visiting = [packed]
    for _ in range(furthest):
        visiting.append(passed_along(visiting[-1], "ep", 1))
    visiting = jnp.stack(visiting)
    keys = visiting[:, : span * key_groups].reshape(-1, span, key_groups, pair_width)
    keys = keys.transpose(0, 2, 1, 3)
    biases = visiting[:, span * key_groups :].reshape(-1, key_groups, 1, span)
    size = min(span, 256)
    attended = pl.pallas_call(
        attention_kernel,
        grid=(heads,),
        out_shape=jax.ShapeDtypeStruct((heads, span, head_dim), BF16),
        in_specs=[
            pl.BlockSpec(memory_space=pltpu.SMEM),
            pl.BlockSpec((1, span, head_dim), lambda h: (h, 0, 0)),
            pl.BlockSpec((furthest + 1, 1, span, pair_width), lambda h: (0, h // per_group, 0, 0)),
            pl.BlockSpec((furthest + 1, 1, 1, span), lambda h: (0, h // per_group, 0, 0)),
        ],
        out_specs=pl.BlockSpec((1, span, head_dim), lambda h: (h, 0, 0)),
        scratch_shapes=[
            pltpu.VMEM((span // size, size, head_dim), F32),
            pltpu.VMEM((span // size, size, 128), F32),
        ],
        name="attention",
        cost_estimate=pl.CostEstimate(flops=4 * 10**9, bytes_accessed=10**6, transcendentals=0),
    )(
        chain_place.reshape(1),
        queries.reshape(span, heads, head_dim).transpose(1, 0, 2),
        keys,
        biases,
    )
    return attended.transpose(1, 0, 2).reshape(span, heads * head_dim)


def project(attended, out_weight):
    return jnp.dot(attended, out_weight, preferred_element_type=F32).astype(BF16)


def layer_kernel(
    capacity,
    q_ref,
    kv_ref,
    bias_ref,
    x_ref,
    gain_ref,
    routes_ref,
    route_weights_ref,
    out_weight_hbm,
    shared_gate_hbm,
    shared_up_hbm,
    shared_down_hbm,
    gate_hbm,
    up_hbm,
    down_hbm,
    mixer_ref,
    expert_ref,
    gathered,
    gathered_s,
    meta_out,
    meta,
    staged,
    staged_s,
    chosen,
    rows_in,
    rows_in_s,
    sums,
    sums_s,
    line_in,
    line_in_s,
    acc,
    acc_s,
    from_side,
    shared,
    out_weight_v,
    shared_gate_v,
    shared_up_v,
    shared_down_v,
    gate_v,
    up_v,
    down_v,
    kv_next,
    bias_row,
    bias_next,
    values_t,
    biases_t,
    att_total,
    att_kept,
    attended_t,
    terms,
    mixer_in,
    mixer_sum,
    mixer_side,
    load_sem,
    meta_send,
    meta_recv,
    kv_send,
    kv_recv,
    zs_send,
    zs_recv,
    s_send,
    s_recv,
    xa_send,
    xa_recv,
    xr_send,
    xr_recv,
    rz_send,
    rz_recv,
    last_send,
    last_recv,
    m_send,
    m_recv,
):
    count = lax.axis_size("ep")
    tokens, width = x_ref.shape
    columns = piece_columns(width)
    pieces = len(columns)
    cut = columns[0].stop
    items = pieces + 1
    z = lax.axis_index("ep")
    t = lax.axis_index("tp")
    x, c = t // 2, t % 2
    ox, oc = 1 - x, 1 - c
    places = (t, x * 2 + oc, ox * 2 + c, ox * 2 + oc)
    sibling, side = places[1], places[2]
    is_end = (z == 0) | (z == count - 1)

    def inside(zz):
        return (zz >= 0) & (zz < count)

    def copy(src, dst, send, recv, ep, tp):
        return pltpu.make_async_remote_copy(
            src_ref=src,
            dst_ref=dst,
            send_sem=send,
            recv_sem=recv,
            device_id={"ep": ep, "tp": tp},
            device_id_type=MESH,
        )

    def band(r):
        return slice(r * capacity, (r + 1) * capacity)

    loads = {
        name: pltpu.make_async_copy(a, b, load_sem.at[i])
        for i, (name, a, b) in enumerate(
            (
                ("shared_gate", shared_gate_hbm, shared_gate_v),
                ("shared_up", shared_up_hbm, shared_up_v),
                ("shared_down", shared_down_hbm, shared_down_v),
                ("gate", gate_hbm, gate_v),
                ("up", up_hbm, up_v),
                ("down", down_hbm, down_v),
                ("out_weight", out_weight_hbm, out_weight_v),
            )
        )
    }

    barrier = pltpu.get_barrier_semaphore()

    def greet(ep, tp):
        pl.semaphore_signal(barrier, 1, device_id={"ep": ep, "tp": tp}, device_id_type=MESH)

    for step in range(1, count):
        for sx in (0, 2):
            greet((z + step) % count, places[sx])
    for r in (1, 2, 3):
        greet(z, places[r])

    @pl.loop(0, tokens // 16)
    def _(block):
        rows = pl.ds(pl.multiple_of(block * 16, 16), 16)
        wide = x_ref[rows, :].astype(F32)
        mean = jnp.mean(wide * wide, axis=-1, keepdims=True)
        gathered[z, rows, :] = (wide * lax.rsqrt(mean + 1e-06) * gain_ref[...]).astype(BF16)

    lines = lax.broadcasted_iota(jnp.int32, (count * 8, tokens), 0)
    expert = (lines // 8) * 4 + lines % 4
    named = jnp.zeros((count * 8, tokens), F32)
    weight = jnp.zeros((count * 8, tokens), F32)
    for k in range(routes_ref.shape[0]):
        hit = routes_ref[k : k + 1, :] == expert
        named = named + jnp.where(hit, 1.0, 0.0)
        weight = weight + jnp.where(hit, route_weights_ref[k : k + 1, :], 0.0)
    before = lax.broadcasted_iota(jnp.int32, (tokens, tokens), 0) < lax.broadcasted_iota(
        jnp.int32, (tokens, tokens), 1
    )
    slot = jnp.dot(
        named.astype(BF16), jnp.where(before, 1.0, 0.0).astype(BF16), preferred_element_type=F32
    )
    slot = jnp.where(named > 0.5, slot, -1.0)
    meta_out[...] = jnp.where(lines % 8 < 4, slot, weight).reshape(meta_out.shape)
    meta[0, z] = meta_out[z]
    bias_row[...] = jnp.broadcast_to(bias_ref[...].astype(F32), bias_row.shape)

    pl.semaphore_wait(barrier, 2 * (count - 1) + 3)

    def meta_copy(step, sx):
        other = (z + step) % count
        return copy(
            meta_out.at[other],
            meta.at[sx, z],
            meta_send.at[sx, step],
            meta_recv.at[sx, z],
            other,
            places[2 * sx],
        )

    def meta_wait(sx, zz):
        copy(
            meta_out.at[zz], meta.at[sx, zz], meta_send.at[sx, 0], meta_recv.at[sx, zz], z, side
        ).wait_recv()

    def s_move():
        return copy(
            gathered.at[z, :, columns[0]], gathered_s.at[z], s_send.at[0], s_recv.at[0], z, side
        )

    def line(i, zz, item):
        block = gathered_s.at[zz] if item == pieces else gathered.at[zz, :, columns[item]]
        return copy(
            block, block, zs_send.at[i, item, zz], zs_recv.at[item, zz], z + 2 * i - 1, t
        )

    def kv_move(which):
        pair = ((kv_ref, kv_next), (bias_row, bias_next))[which]
        return copy(*pair, kv_send.at[which], kv_recv.at[which], z + 1, t)

    chain = count // max(1, count // 4)

    def chain_place(zz):
        return jnp.minimum((zz + 2) % chain, zz)

    sends_kv = (z + 1 < count) & (chain_place(z + 1) >= 1)
    takes_kv = chain_place(z) >= 1

    for step in range(1, count):
        for sx in range(2):
            meta_copy(step, sx).start()
    meta_copy(0, 1).start()
    s_move().start()
    for item in range(pieces):
        for i in range(2):

            @pl.when(inside(z + 2 * i - 1))
            def _():
                line(i, z, item).start()

    slots = lax.broadcasted_iota(jnp.int32, (capacity, tokens), 0).astype(F32)

    def one_hot(sx, zz, rels):
        return jnp.concatenate(
            [jnp.where(meta[sx, zz, pl.ds(places[r], 1), :] == slots, 1.0, 0.0) for r in rels],
            axis=0,
        ).astype(BF16)

    def spreader(sx, zz, rels):
        weights = jnp.concatenate(
            [
                jnp.where(
                    meta[sx, zz, pl.ds(places[r], 1), :] == slots,
                    meta[sx, zz, pl.ds(4 + places[r], 1), :],
                    0.0,
                )
                for r in rels
            ],
            axis=0,
        )
        high = weights.astype(BF16)
        return high, (weights - high.astype(F32)).astype(BF16)

    def spread(pair, rows):
        return sum(
            lax.dot_general(half, rows, (((0,), (0,)), ((), ())), preferred_element_type=F32)
            for half in pair
        )

    def row_copy(r, zz, p):
        if p == 0 and r == 3:
            return copy(
                staged_s.at[zz],
                chosen.at[zz, band(3), columns[0]],
                xa_send.at[r, p, zz],
                xa_recv.at[r, p, zz],
                z,
                sibling,
            )
        return copy(
            staged.at[zz, band(r - 1), columns[p]],
            chosen.at[zz, band(r), columns[p]],
            xa_send.at[r, p, zz],
            xa_recv.at[r, p, zz],
            z,
            places[r],
        )

    def pick(zz, p):
        rels = (0, 1) if p == 0 else (0, 1, 2, 3)
        picked = jnp.dot(
            one_hot(0, zz, rels), gathered[zz, :, columns[p]], preferred_element_type=F32
        ).astype(BF16)
        staged[zz, : (len(rels) - 1) * capacity, columns[p]] = picked[capacity:]
        chosen[zz, band(0), columns[p]] = picked[:capacity]
        for r in rels[:0:-1]:
            row_copy(r, zz, p).start()

    def pick_s(zz):
        picked = jnp.dot(
            one_hot(1, zz, (0, 1)), gathered_s[zz], preferred_element_type=F32
        ).astype(BF16)
        staged_s[zz] = picked[capacity:]
        chosen[zz, band(2), columns[0]] = picked[:capacity]
        row_copy(3, zz, 0).start()

    for p in (*range(1, pieces), 0):
        pick(z, p)
    s_move().wait_recv()
    for i in range(2):

        @pl.when(inside(z + 2 * i - 1))
        def _():
            line(i, z, pieces).start()

    @pl.when(sends_kv)
    def _():
        kv_move(1).start()
        kv_move(0).start()

    for load in loads.values():
        load.start()
    meta_wait(1, z)
    pick_s(z)

    span = kv_ref.shape[0]
    head_dim = kv_ref.shape[1] // 2
    heads = q_ref.shape[0] // head_dim
    size = min(span, 256)
    tiles = span // size
    key_line = lax.broadcasted_iota(jnp.int32, (size, size), 0)
    query_line = lax.broadcasted_iota(jnp.int32, (size, size), 1)

    def prepare(b, kv, bias):
        values_t[b] = kv[...].astype(F32).T[head_dim:, :].astype(BF16)
        biases_t[b] = jnp.broadcast_to(bias[0:1, :], (128, span)).T

    def tile(b, kv, h, i, j, state):
        there = slice(j * size, (j + 1) * size)
        diagonal = b == 0 and i == j
        later = jnp.where(key_line < query_line, 1.0, 0.0).astype(BF16)
        q = q_ref[pl.ds(pl.multiple_of(h * head_dim, head_dim), head_dim), i * size : (i + 1) * size]
        logits = jnp.dot(kv[there, :head_dim], q, preferred_element_type=F32) * 0.125
        logits = logits + biases_t[b, there, 0:1]
        log_sig = jnp.minimum(logits, 0.0) - jnp.log(1.0 + jnp.exp(-jnp.abs(logits)))
        keep = log_sig - logits
        if diagonal:
            keep = jnp.where(key_line < query_line, keep, 0.0)
        high = keep.astype(BF16)
        low = (keep - high.astype(F32)).astype(BF16)
        after = jnp.dot(later, high, preferred_element_type=F32)
        after = after + jnp.dot(later, low, preferred_element_type=F32)
        weights = jnp.exp(log_sig + after + state[1])
        if diagonal:
            weights = jnp.where(key_line < query_line, weights, 0.0)
        part = jnp.dot(values_t[b, :, there], weights.astype(BF16), preferred_element_type=F32)
        return state[0] + part, state[1] + jnp.sum(keep, axis=0, keepdims=True)

    def attend_own():
        prepare(0, kv_ref, bias_row)

        @pl.loop(0, heads)
        def _(h):
            for i in range(tiles):
                state = (jnp.zeros((head_dim, size), F32), jnp.zeros((1, size), F32))
                for j in range(i, -1, -1):
                    state = tile(0, kv_ref, h, i, j, state)
                att_total[h, i] = state[0]
                att_kept[h, i] = jnp.broadcast_to(state[1], att_kept.shape[2:])

    def attend_next():
        @pl.when(takes_kv)
        def _():
            for which in range(2):
                kv_move(which).wait_recv()
            prepare(1, kv_next, bias_next)

            @pl.loop(0, heads)
            def _(h):
                for i in range(tiles):
                    state = (att_total[h, i], att_kept[h, i, 0:1, :])
                    for j in range(tiles - 1, -1, -1):
                        state = tile(1, kv_next, h, i, j, state)
                    att_total[h, i] = state[0]

    def mixer_pair(k):
        return copy(
            terms.at[3 - 2 * k], mixer_in.at[k], m_send.at[k], m_recv.at[k], z, sibling
        )

    def mixer_move():
        return copy(mixer_sum, mixer_side, m_send.at[2], m_recv.at[2], z, side)

    def project():
        for h in range(heads):
            for i in range(tiles):
                attended_t[h * head_dim : (h + 1) * head_dim, i * size : (i + 1) * size] = (
                    att_total[h, i].astype(BF16)
                )
        loads["out_weight"].wait()
        for r in (3, 1, 2, 0):
            own = pl.ds(pl.multiple_of(places[r] * tokens, tokens), tokens)
            terms[r] = lax.dot_general(
                attended_t[:, own],
                out_weight_v[...],
                (((0,), (0,)), ((), ())),
                preferred_element_type=F32,
            ).astype(BF16)
            if r % 2:
                mixer_pair((3 - r) // 2).start()
        mixer_pair(0).wait_recv()
        mixer_sum[...] = (terms[2].astype(F32) + mixer_in[0].astype(F32)).astype(BF16)

    def shared_expert():
        for name in ("shared_gate", "shared_up", "shared_down"):
            loads[name].wait()
        hidden_gate = jnp.dot(gathered[z], shared_gate_v[...], preferred_element_type=F32)
        hidden_up = jnp.dot(gathered[z], shared_up_v[...], preferred_element_type=F32)
        hidden = (hidden_gate / (1.0 + jnp.exp(-hidden_gate)) * hidden_up).astype(BF16)
        shared[...] = jnp.dot(hidden, shared_down_v[...], preferred_element_type=F32)

    def both(body):
        @pl.loop(0, 2)
        def _(i):
            body(i)

    def arrive(distance, item):
        def body(i):
            zz = z - (2 * i - 1) * distance

            @pl.when(inside(zz))
            def _():
                line(i, zz, item).wait_recv()

                @pl.when(inside(z + 2 * i - 1))
                def _():
                    line(i, zz, item).start()

                if item == 0:
                    meta_wait(0, zz)
                if item == pieces:
                    meta_wait(1, zz)
                    pick_s(zz)
                else:
                    pick(zz, item)

        both(body)

    def result_copy(r, zz, p):
        if p == 0 and r == 3:
            destination, device = rows_in_s.at[zz, band(1)], sibling
        else:
            destination, device = rows_in.at[zz, band(r), columns[p]], places[r]
        return copy(
            chosen.at[zz, band(r), columns[p]],
            destination,
            xr_send.at[r, p, zz],
            xr_recv.at[r, p, zz],
            z,
            device,
        )

    def crossing(p):
        return (1, 3) if p == 0 else (3, 2, 1)

    def feed_forward(zz, send):
        for p in range(pieces):
            for r in crossing(p):
                row_copy(r, zz, p).wait_recv()
        gate = jnp.dot(chosen[zz], gate_v[...], preferred_element_type=F32)
        up = jnp.dot(chosen[zz], up_v[...], preferred_element_type=F32)
        hidden = (gate / (1.0 + jnp.exp(-gate)) * up).astype(BF16)
        for p in range(pieces):
            rows = jnp.dot(hidden, down_v[:, columns[p]], preferred_element_type=F32).astype(BF16)
            chosen[zz, :, columns[p]] = rows
            rows_in[zz, band(0), columns[p]] = rows[band(0)]
            if p == 0:
                rows_in_s[zz, band(0)] = rows[band(2)]
            if send:
                for r in crossing(p):
                    result_copy(r, zz, p).start()

    def feed_forward_at(distance):
        def body(i):
            zz = z - (2 * i - 1) * distance

            @pl.when(inside(zz))
            def _():
                feed_forward(zz, True)

        both(body)

    def send_own_results():
        for p in range(pieces):
            for r in crossing(p):
                result_copy(r, z, p).start()

    def back(i, target, item):
        if item == pieces:
            source, destination = sums_s.at[target], line_in_s.at[i, target]
        else:
            source = sums.at[target, :, columns[item]]
            destination = line_in.at[i, target, :, columns[item]]
        return copy(
            source,
            destination,
            rz_send.at[item, target],
            rz_recv.at[i, item, target],
            z + 2 * i - 1,
            t,
        )

    def total_of(zz, item):
        if item == pieces:
            result_copy(3, zz, 0).wait_recv()
            acc_s[...] = spread(spreader(1, zz, (0, 1)), rows_in_s[zz])
        elif item == 0:
            result_copy(1, zz, 0).wait_recv()
            acc[:, columns[0]] = spread(
                spreader(0, zz, (0, 1)), rows_in[zz, : 2 * capacity, columns[0]]
            )
        else:
            for r in crossing(item):
                result_copy(r, zz, item).wait_recv()
            acc[:, columns[item]] = spread(
                spreader(0, zz, (0, 1, 2, 3)), rows_in[zz, :, columns[item]]
            )

    def take_line(i, zz, item):
        back(i, zz, item).wait_recv()
        if item == pieces:
            acc_s[...] += line_in_s[i, zz].astype(F32)
        else:
            acc[:, columns[item]] += line_in[i, zz, :, columns[item]].astype(F32)

    item_order = (pieces, *range(pieces))

    def stage(s):
        for item in item_order:

            def body(i):
                up = 2 * i - 1
                target = s * i + (count - 1 - s) * (1 - i)

                @pl.when(up * (target - z) > 0)
                def _():
                    total_of(target, item)

                    @pl.when(inside(z - up))
                    def _():
                        take_line(i, target, item)

                    if item == pieces:
                        sums_s[target] = acc_s[...].astype(BF16)
                    else:
                        sums[target, :, columns[item]] = acc[:, columns[item]].astype(BF16)
                    back(i, target, item).start()

            both(body)

    attend_own()
    for distance in range(1, count):
        arrive(distance, 0)
        arrive(distance, 1)
        if distance == 1:
            shared_expert()
        if distance >= 2:
            feed_forward_at(distance - 1)
        if distance == 2:
            project()
        if distance == count - 1:

            @pl.when(jnp.logical_not(is_end))
            def _():
                send_own_results()
                mixer_move().start()

        if distance >= 3:
            stage(distance - 2)
        for item in range(2, items):
            arrive(distance, item)
        if distance == 1:
            for name in ("gate", "up", "down"):
                loads[name].wait()
            feed_forward(z, False)

            @pl.when(is_end)
            def _():
                send_own_results()

            attend_next()

    stage(count - 2)
    feed_forward_at(count - 1)

    @pl.when(is_end)
    def _():
        mixer_move().start()

    stage(count - 1)

    def last_move():
        return copy(sums_s.at[z], from_side, last_send.at[0], last_recv.at[0], z, side)

    for item in item_order:
        total_of(z, item)

        def body(i):
            @pl.when(inside(z - (2 * i - 1)))
            def _():
                take_line(i, z, item)

        both(body)
        if item == pieces:
            sums_s[z] = acc_s[...].astype(BF16)
            last_move().start()
        elif item > 0:
            expert_ref[:, columns[item]] = (
                acc[:, columns[item]] + shared[:, columns[item]]
            ).astype(BF16)
    last_move().wait_recv()
    expert_ref[:, columns[0]] = (
        acc[:, columns[0]] + from_side[...].astype(F32) + shared[:, columns[0]]
    ).astype(BF16)

    mixer_pair(1).wait_recv()
    mixer_move().wait_recv()
    mixer_ref[...] = (
        terms[0].astype(F32) + mixer_in[1].astype(F32) + mixer_side[...].astype(F32)
    ).astype(BF16)

    for step in range(1, count):
        for sx in range(2):
            meta_copy(step, sx).wait_send()
    meta_copy(0, 1).wait_send()
    s_move().wait_send()

    @pl.when(sends_kv)
    def _():
        for which in range(2):
            kv_move(which).wait_send()

    for k in range(2):
        mixer_pair(k).wait_send()
    mixer_move().wait_send()
    last_move().wait_send()

    @pl.loop(0, count)
    def _(zz):
        for p in range(pieces):
            for r in crossing(p):
                row_copy(r, zz, p).wait_send()
                result_copy(r, zz, p).wait_send()
        for item in range(items):
            for i in range(2):
                up = 2 * i - 1

                @pl.when((up * (z - zz) >= 0) & inside(z + up))
                def _():
                    line(i, zz, item).wait_send()

                @pl.when(up * (zz - z) > 0)
                def _():
                    back(i, zz, item).wait_send()


def piece_columns(width):
    unit = width // 8
    edges = (0, 1, 4, 6, 8)
    return [slice(a * unit, b * unit) for a, b in zip(edges, edges[1:])]


def layer(
    queries,
    key_value,
    key_bias,
    out_weight,
    expert_input,
    norm_gain,
    routes,
    route_weights,
    routed_parts,
    shared_parts,
    capacity,
):
    tokens, width = expert_input.shape
    count = lax.axis_size("ep")
    columns = piece_columns(width)
    pieces, cut = len(columns), columns[0].stop
    items = pieces + 1
    span, _, pair_width = key_value.shape
    head_dim = pair_width // 2
    heads = queries.shape[1] // head_dim
    size = min(span, 256)
    hidden = routed_parts[0].shape[1]
    band = 4 * capacity
    dma = pltpu.SemaphoreType.DMA
    vmem = pl.BlockSpec(memory_space=pltpu.VMEM)
    hbm = pl.BlockSpec(memory_space=pl.ANY)
    buffers = [
        ((count, tokens, width), BF16),
        ((count, tokens, cut), BF16),
        ((count, 8, tokens), F32),
        ((2, count, 8, tokens), F32),
        ((count, 3 * capacity, width), BF16),
        ((count, capacity, cut), BF16),
        ((count, band, width), BF16),
        ((count, band, width), BF16),
        ((count, 2 * capacity, cut), BF16),
        ((count, tokens, width), BF16),
        ((count, tokens, cut), BF16),
        ((2, count, tokens, width), BF16),
        ((2, count, tokens, cut), BF16),
        ((tokens, width), F32),
        ((tokens, cut), F32),
        ((tokens, cut), BF16),
        ((tokens, width), F32),
        (out_weight.shape, BF16),
        (shared_parts[0].shape, BF16),
        (shared_parts[1].shape, BF16),
        (shared_parts[2].shape, BF16),
        ((width, hidden), BF16),
        ((width, hidden), BF16),
        ((hidden, width), BF16),
        ((span, pair_width), BF16),
        ((8, span), F32),
        ((8, span), F32),
        ((2, head_dim, span), BF16),
        ((2, span, 128), F32),
        ((heads, span // size, head_dim, size), F32),
        ((heads, span // size, 8, size), F32),
        ((heads * head_dim, span), BF16),
        ((4, tokens, width), BF16),
        ((2, tokens, width), BF16),
        ((tokens, width), BF16),
        ((tokens, width), BF16),
    ]
    semaphores = [
        (7,),
        (2, count),
        (2, count),
        (2,),
        (2,),
        (2, items, count),
        (items, count),
        (1,),
        (1,),
        (4, pieces, count),
        (4, pieces, count),
        (4, pieces, count),
        (4, pieces, count),
        (items, count),
        (2, items, count),
        (1,),
        (1,),
        (3,),
        (3,),
    ]
    return pl.pallas_call(
        lambda *refs: layer_kernel(capacity, *refs),
        out_shape=[jax.ShapeDtypeStruct((tokens, width), BF16)] * 2,
        in_specs=[vmem] * 7 + [hbm] * 7,
        out_specs=[vmem] * 2,
        scratch_shapes=[pltpu.VMEM(*b) for b in buffers] + [dma(s) for s in semaphores],
        compiler_params=pltpu.CompilerParams(
            collective_id=0, has_side_effects=True, vmem_limit_bytes=60 * 2**20
        ),
        name="layer",
        cost_estimate=pl.CostEstimate(flops=10**10, bytes_accessed=2 * 10**7, transcendentals=0),
    )(
        queries.T,
        key_value.reshape(span, pair_width),
        key_bias,
        expert_input,
        norm_gain.reshape(1, width),
        routes.T,
        route_weights.T,
        out_weight,
        *shared_parts,
        *routed_parts,
    )


def expert_rows(arrived, gate_weight, up_weight, down_weight):
    sources, capacity, model_width = arrived.shape
    flat_rows = arrived.reshape(sources * capacity, model_width)
    gate_part = jnp.dot(flat_rows, gate_weight[0], preferred_element_type=jnp.float32)
    up_part = jnp.dot(flat_rows, up_weight[0], preferred_element_type=jnp.float32)
    hidden = (jax.nn.silu(gate_part) * up_part).astype(jnp.bfloat16)
    result = jnp.dot(hidden, down_weight[0], preferred_element_type=jnp.float32).astype(
        jnp.bfloat16
    )
    return result.reshape(sources, capacity, model_width)


def experts_half(
    expert_input,
    norm_gain,
    routes,
    route_weights,
    gate_weight,
    up_weight,
    down_weight,
    shared_gate,
    shared_up,
    shared_down,
):
    tokens, top_count = routes.shape
    model_width = expert_input.shape[1]
    ep_count = lax.axis_size("ep")
    tp_count = lax.axis_size("tp")
    experts = ep_count * tp_count
    capacity = max(2, 3 * tokens * top_count // (2 * experts))
    widened = expert_input.astype(jnp.float32)
    normed = (
        widened * lax.rsqrt(jnp.mean(widened * widened, axis=-1, keepdims=True) + 1e-06) * norm_gain
    ).astype(jnp.bfloat16)
    flat_routes = routes.reshape(-1)
    one_hot = (flat_routes[:, None] == jnp.arange(experts, dtype=jnp.int32)[None, :]).astype(
        jnp.int32
    )
    before = jnp.cumsum(one_hot, axis=0) - one_hot
    slot_index = jnp.sum(before * one_hot, axis=1)
    target = flat_routes * capacity + slot_index
    picker = (jnp.arange(experts * capacity, dtype=jnp.int32)[:, None] == target[None, :]).astype(
        jnp.bfloat16
    )
    picker = jnp.sum(picker.reshape(experts * capacity, tokens, top_count), axis=2)
    outgoing = jnp.dot(picker, normed, preferred_element_type=jnp.float32).astype(jnp.bfloat16)
    outgoing = outgoing.reshape(experts, capacity, model_width)
    came_back = lax.all_to_all(
        expert_rows(
            lax.all_to_all(outgoing, ("ep", "tp"), split_axis=0, concat_axis=0, tiled=True),
            gate_weight,
            up_weight,
            down_weight,
        ),
        ("ep", "tp"),
        split_axis=0,
        concat_axis=0,
        tiled=True,
    )
    back_rows = came_back.reshape(experts * capacity, model_width)
    picked = jnp.take(back_rows, target, axis=0).reshape(tokens, top_count, model_width)
    routed = jnp.sum(picked.astype(jnp.float32) * route_weights[:, :, None], axis=1)
    shared_hidden = (
        jax.nn.silu(jnp.dot(normed, shared_gate, preferred_element_type=jnp.float32))
        * jnp.dot(normed, shared_up, preferred_element_type=jnp.float32)
    ).astype(jnp.bfloat16)
    shared_term = jnp.dot(shared_hidden, shared_down, preferred_element_type=jnp.float32)
    return (routed + shared_term).astype(jnp.bfloat16)


def per_device(
    queries,
    key_value,
    key_bias,
    out_weight,
    expert_input,
    norm_gain,
    routes,
    route_weights,
    gate_weight,
    up_weight,
    down_weight,
    shared_gate,
    shared_up,
    shared_down,
):
    tokens, top_count = routes.shape
    span, key_groups, pair_width = key_value.shape
    width = expert_input.shape[1]
    ep_count, tp_count = lax.axis_size("ep"), lax.axis_size("tp")
    experts = ep_count * tp_count
    capacity = max(2, 3 * tokens * top_count // (2 * experts))
    fits = experts * tokens * width * 2 <= 8 * 2**20 and capacity % 16 == 0 and ep_count >= 3
    whole = tp_count == 4 and span == tp_count * tokens and tokens == 128
    heads_fit = key_groups == 1 and pair_width == 128 and width % 1024 == 0
    if fits and whole and heads_fit and furthest_place(ep_count) <= 1:
        return tuple(
            layer(
                queries,
                key_value,
                key_bias,
                out_weight,
                expert_input,
                norm_gain,
                routes,
                route_weights,
                (gate_weight[0], up_weight[0], down_weight[0]),
                (shared_gate, shared_up, shared_down),
                capacity,
            )
        )
    terms = project(attend(queries, key_value, key_bias), out_weight)
    mixer_output = lax.psum_scatter(terms, "tp", scatter_dimension=0, tiled=True)
    expert_output = experts_half(
        expert_input,
        norm_gain,
        routes,
        route_weights,
        gate_weight,
        up_weight,
        down_weight,
        shared_gate,
        shared_up,
        shared_down,
    )
    return (mixer_output, expert_output)


def solution(mesh):
    placed = (
        P(("grp", "ep"), "tp"),
        P(("grp", "ep"), "tp", None),
        P("tp", ("grp", "ep")),
        P("tp", None),
        P(("grp", "ep", "tp"), None),
        P(),
        P(("grp", "ep", "tp"), None),
        P(("grp", "ep", "tp"), None),
        P(("ep", "tp"), None, None),
        P(("ep", "tp"), None, None),
        P(("ep", "tp"), None, None),
        P(),
        P(),
        P(),
    )
    return jax.shard_map(
        per_device,
        mesh=mesh,
        in_specs=placed,
        out_specs=(P(("grp", "ep", "tp"), None), P(("grp", "ep", "tp"), None)),
        check_vma=False,
    )
```

time: 148 us -> 135 us (0.912); the launches traced: 148 us -> 133 us
  other arithmetic: 7.79 us -> 0 us
  starting transfers between devices: 4.96 us -> 0 us
  Pallas kernels: 125 us -> 128 us
  local copies, waits for them, and re-layouts: 6.43 us -> 3.76 us
  matrix products: 2.24 us -> 0 us
    ppermute x1 -> x0, starting transfers between devices: 4.96 us -> none  [passed_along(): return lax.ppermute(block, axis, route)]
    pallas_call x2 -> x1, Pallas kernels: 125 us -> 128 us  [layer(): pl.pallas_call(lambda *refs: layer_kernel(capacity, *refs), out_shape=[ja...]
    dot_general x2 -> x0, matrix products: 2.24 us -> none  [the longest x1 2.1 us: project(): jnp.dot(attended, out_weight, preferred_element_type=F32).astype(BF16)]
    convert_element_type x1 -> x0, other arithmetic: 2.04 us -> none  [normalise(): return (widened * lax.rsqrt(jnp.mean(widened * widened, axis=-1, keepdims...]
    reduce_sum x2 -> x0, other arithmetic: 1.94 us -> none  [the longest x1 1.23 us: normalise(): jnp.mean(widened * widened, axis=-1, keepdims=True) + 1e-06]
    reshape x2 -> x0, local copies, waits for them, and re-layouts: 1.51 us -> none  [the longest x1 0.92 us: attend(): queries.reshape(span, heads, head_dim).transpose(1, 0, 2)]
    unnamed x6 -> x2, local copies, waits for them, and re-layouts: 3.78 us -> 3.76 us
  transfers between devices with their start and end apart: 1 -> 0, of which waited for: 0 -> 0; matrix products, arithmetic and copies ran while one was open for 4% -> 0% of each run, Pallas kernels for 0% -> 0%
where the time goes in v1:
time: 135 us; the launch traced here: 133 us
  Pallas kernels  128 us (95%)
  local copies, waits for them, and re-layouts  3.76 us (3%)
    pallas_call x1, Pallas kernels, layer(): pl.pallas_call(lambda *refs: layer_kernel(capacity, *refs), out_shape=[ja...  128 us
    unnamed x2, local copies, waits for them, and re-layouts  3.76 us

profile of v1, /device:TPU:0, one launch (start us, length us, event | category | flops | bytes accessed | tf_op | source)
XLA Modules:
  0.0 132.6 jit_solution(3983739620201658267)
XLA Ops:
  0.6 128.2 %layer.1 = (bf16[128,2048]{1,0:T(8,128)(2,1)}, bf16[128,2048]{1,0:T(8,128)(2,1)}) custom-call(bf16[192,512]{1,0:T(8,128)(2,1)} %bitcast.11, bf16[512,128]{1,0:T(8,128)(2,1)} %bitcast.12, bf16[1,512]{1,0:T(2,128)(2,1)} %refs_2_.1, bf16[128,2048]{1,0:T(8,128)(2,1)} %refs_3_.1, f32[1,2048]{1,0:T(1,128)} %bitcast.13, s32[4,128]{1,0:T(4,128)} %bitcast.14, ...), custom_call_target="tpu_custom_call" | custom-call | flops 10000000000 | bytes 20000000 | tf_op jit(solution)/shard_map/layer/pallas_call | solution.py:864
  128.9 1.9 %copy.18 = bf16[128,2048]{1,0:T(8,128)(2,1)} copy(bf16[128,2048]{1,0:T(8,128)(2,1)} %get-tuple-element.4) | data formatting | bytes 1048576
  130.8 1.9 %copy.19 = bf16[128,2048]{1,0:T(8,128)(2,1)} copy(bf16[128,2048]{1,0:T(8,128)(2,1)} %get-tuple-element.5) | data formatting | bytes 1048576

commit v2 on v1

--- a/solution.py
+++ b/solution.py
@@ -314,9 +314,10 @@
         )
 
     def line(i, zz, item):
-        block = gathered_s.at[zz] if item == pieces else gathered.at[zz, :, columns[item]]
+        small = 1 if item == pieces else 0
+        block = gathered_s.at[zz] if small else gathered.at[zz, :, columns[item]]
         return copy(
-            block, block, zs_send.at[i, item, zz], zs_recv.at[item, zz], z + 2 * i - 1, t
+            block, block, zs_send.at[i, small, zz], zs_recv.at[item, zz], z + 2 * i - 1, t
         )
 
     def kv_move(which):
@@ -377,16 +378,16 @@
             return copy(
                 staged_s.at[zz],
                 chosen.at[zz, band(3), columns[0]],
-                xa_send.at[r, p, zz],
-                xa_recv.at[r, p, zz],
+                xa_send.at[r],
+                xa_recv.at[r, zz],
                 z,
                 sibling,
             )
         return copy(
             staged.at[zz, band(r - 1), columns[p]],
             chosen.at[zz, band(r), columns[p]],
-            xa_send.at[r, p, zz],
-            xa_recv.at[r, p, zz],
+            xa_send.at[r],
+            xa_recv.at[r, zz],
             z,
             places[r],
         )
@@ -473,14 +474,15 @@
                 att_total[h, i] = state[0]
                 att_kept[h, i] = jnp.broadcast_to(state[1], att_kept.shape[2:])
 
-    def attend_next():
+    def attend_next(first, low, high):
         @pl.when(takes_kv)
         def _():
-            for which in range(2):
-                kv_move(which).wait_recv()
-            prepare(1, kv_next, bias_next)
-
-            @pl.loop(0, heads)
+            if first:
+                for which in range(2):
+                    kv_move(which).wait_recv()
+                prepare(1, kv_next, bias_next)
+
+            @pl.loop(low, high)
             def _(h):
                 for i in range(tiles):
                     state = (att_total[h, i], att_kept[h, i, 0:1, :])
@@ -559,19 +561,27 @@
         return copy(
             chosen.at[zz, band(r), columns[p]],
             destination,
-            xr_send.at[r, p, zz],
+            xr_send.at[r],
             xr_recv.at[r, p, zz],
             z,
             device,
         )
 
+    def reach(r):
+        return slice(cut if r == 2 else 0, width)
+
     def crossing(p):
         return (1, 3) if p == 0 else (3, 2, 1)
 
-    def feed_forward(zz, send):
+    def send_results(zz):
         for p in range(pieces):
             for r in crossing(p):
-                row_copy(r, zz, p).wait_recv()
+                result_copy(r, zz, p).start()
+
+    def feed_forward(zz, send):
+        for r in (1, 2, 3):
+            arrived = chosen.at[zz, band(r), reach(r)]
+            copy(arrived, arrived, xa_send.at[r], xa_recv.at[r, zz], z, sibling).wait_recv()
         gate = jnp.dot(chosen[zz], gate_v[...], preferred_element_type=F32)
         up = jnp.dot(chosen[zz], up_v[...], preferred_element_type=F32)
         hidden = (gate / (1.0 + jnp.exp(-gate)) * up).astype(BF16)
@@ -581,6 +591,8 @@
             rows_in[zz, band(0), columns[p]] = rows[band(0)]
             if p == 0:
                 rows_in_s[zz, band(0)] = rows[band(2)]
+
+
             if send:
                 for r in crossing(p):
                     result_copy(r, zz, p).start()
@@ -594,11 +606,6 @@
                 feed_forward(zz, True)
 
         both(body)
-
-    def send_own_results():
-        for p in range(pieces):
-            for r in crossing(p):
-                result_copy(r, z, p).start()
 
     def back(i, target, item):
         if item == pieces:
@@ -609,7 +616,7 @@
         return copy(
             source,
             destination,
-            rz_send.at[item, target],
+            rz_send.at[1 if item == pieces else 0, target],
             rz_recv.at[i, item, target],
             z + 2 * i - 1,
             t,
@@ -640,66 +647,75 @@
 
     item_order = (pieces, *range(pieces))
 
+    near = jnp.where(2 * z < count, 1, 0)
+
+    def stage_item(s, i, item):
+        up = 2 * i - 1
+        target = s * i + (count - 1 - s) * (1 - i)
+
+        @pl.when(up * (target - z) > 0)
+        def _():
+            total_of(target, item)
+
+            @pl.when(inside(z - up))
+            def _():
+                take_line(i, target, item)
+
+            if item == pieces:
+                sums_s[target] = acc_s[...].astype(BF16)
+            else:
+                sums[target, :, columns[item]] = acc[:, columns[item]].astype(BF16)
+            back(i, target, item).start()
+
     def stage(s):
-        for item in item_order:
-
-            def body(i):
-                up = 2 * i - 1
-                target = s * i + (count - 1 - s) * (1 - i)
-
-                @pl.when(up * (target - z) > 0)
+        for k in range(items + 2):
+            if k < items:
+                stage_item(s, near, item_order[k])
+            if k >= 2:
+                stage_item(s, 1 - near, item_order[k - 2])
+
+    attend_own()
+    arrive(1, 0)
+    arrive(1, 1)
+    shared_expert()
+    for item in range(2, items):
+        arrive(1, item)
+    for name in ("gate", "up", "down"):
+        loads[name].wait()
+    feed_forward(z, False)
+    for distance in range(2, count):
+        last = distance == count - 1
+        if not last:
+            pl.when(is_end)(lambda: feed_forward_at(distance - 1))
+        for item in range(items):
+            if last and item == 3:
+                feed_forward_at(distance - 1)
+
+                @pl.when(jnp.logical_not(is_end))
                 def _():
-                    total_of(target, item)
-
-                    @pl.when(inside(z - up))
-                    def _():
-                        take_line(i, target, item)
-
-                    if item == pieces:
-                        sums_s[target] = acc_s[...].astype(BF16)
-                    else:
-                        sums[target, :, columns[item]] = acc[:, columns[item]].astype(BF16)
-                    back(i, target, item).start()
-
-            both(body)
-
-    attend_own()
-    for distance in range(1, count):
-        arrive(distance, 0)
-        arrive(distance, 1)
-        if distance == 1:
-            shared_expert()
-        if distance >= 2:
-            feed_forward_at(distance - 1)
-        if distance == 2:
-            project()
-        if distance == count - 1:
-
-            @pl.when(jnp.logical_not(is_end))
-            def _():
-                send_own_results()
-                mixer_move().start()
-
-        if distance >= 3:
-            stage(distance - 2)
-        for item in range(2, items):
+                    send_results(z)
+
+            if distance == 2 and item in (2, 4):
+                attend_next(item == 2, 0 if item == 2 else heads // 2, heads // 2 if item == 2 else heads - 1)
+            if last and item == 2:
+                attend_next(False, heads - 1, heads)
             arrive(distance, item)
-        if distance == 1:
-            for name in ("gate", "up", "down"):
-                loads[name].wait()
-            feed_forward(z, False)
-
-            @pl.when(is_end)
-            def _():
-                send_own_results()
-
-            attend_next()
+        if not last:
+            pl.when(jnp.logical_not(is_end))(lambda: feed_forward_at(distance - 1))
+            stage(distance - 1)
+
+    @pl.when(jnp.logical_not(is_end))
+    def _():
+        project()
+        mixer_move().start()
 
     stage(count - 2)
     feed_forward_at(count - 1)
 
     @pl.when(is_end)
     def _():
+        send_results(z)
+        project()
         mixer_move().start()
 
     stage(count - 1)
@@ -750,28 +766,36 @@
     mixer_move().wait_send()
     last_move().wait_send()
 
+    for r in (1, 2, 3):
+        for sent, send in (
+            (staged.at[:, band(r - 1), reach(r)], xa_send),
+            (chosen.at[:, band(r), reach(r)], xr_send),
+        ):
+            copy(sent, sent, send.at[r], xa_recv.at[r, 0], z, sibling).wait_send()
+
     @pl.loop(0, count)
     def _(zz):
-        for p in range(pieces):
-            for r in crossing(p):
-                row_copy(r, zz, p).wait_send()
-                result_copy(r, zz, p).wait_send()
-        for item in range(items):
+        for small in range(2):
+            gather, reduce = ((gathered, sums), (gathered_s, sums_s))[small]
             for i in range(2):
                 up = 2 * i - 1
 
                 @pl.when((up * (z - zz) >= 0) & inside(z + up))
                 def _():
-                    line(i, zz, item).wait_send()
-
-                @pl.when(up * (zz - z) > 0)
-                def _():
-                    back(i, zz, item).wait_send()
+                    sent = gather.at[zz]
+                    copy(
+                        sent, sent, zs_send.at[i, small, zz], zs_recv.at[0, zz], z, sibling
+                    ).wait_send()
+
+            @pl.when(zz != z)
+            def _():
+                sent = reduce.at[zz]
+                copy(sent, sent, rz_send.at[small, zz], zs_recv.at[0, zz], z, sibling).wait_send()
 
 
 def piece_columns(width):
-    unit = width // 8
-    edges = (0, 1, 4, 6, 8)
+    unit = width // 16
+    edges = (0, 2, 5, 8, 10, 12, 14, 16)
     return [slice(a * unit, b * unit) for a, b in zip(edges, edges[1:])]
 
 
@@ -846,15 +870,15 @@
         (2, count),
         (2,),
         (2,),
-        (2, items, count),
+        (2, 2, count),
         (items, count),
         (1,),
         (1,),
+        (4,),
+        (4, count),
+        (4,),
         (4, pieces, count),
-        (4, pieces, count),
-        (4, pieces, count),
-        (4, pieces, count),
-        (items, count),
+        (2, count),
         (2, items, count),
         (1,),
         (1,),
@@ -863,7 +887,7 @@
     ]
     return pl.pallas_call(
         lambda *refs: layer_kernel(capacity, *refs),
-        out_shape=[jax.ShapeDtypeStruct((tokens, width), BF16)] * 2,
+        out_shape=[pltpu.VMEM((tokens, width), BF16)] * 2,
         in_specs=[vmem] * 7 + [hbm] * 7,
         out_specs=[vmem] * 2,
         scratch_shapes=[pltpu.VMEM(*b) for b in buffers] + [dma(s) for s in semaphores],

time: 135 us -> 94 us (0.70); the launches traced: 133 us -> 93.9 us
  Pallas kernels: 128 us -> 91.7 us
  local copies, waits for them, and re-layouts: 3.76 us -> 1.59 us
    pallas_call x1, Pallas kernels: 128 us -> 91.7 us  [layer(): pl.pallas_call(lambda *refs: layer_kernel(capacity, *refs), out_shape=[pl...]
    unnamed x2, local copies, waits for them, and re-layouts: 3.76 us -> 1.59 us
where the time goes in v2:
time: 94 us; the launch traced here: 93.9 us
  Pallas kernels  91.7 us (98%)
  local copies, waits for them, and re-layouts  1.59 us (2%)
    pallas_call x1, Pallas kernels, layer(): pl.pallas_call(lambda *refs: layer_kernel(capacity, *refs), out_shape=[pl...  91.7 us

profile of v2, /device:TPU:0, one launch (start us, length us, event | category | flops | bytes accessed | tf_op | source)
XLA Modules:
  0.0 93.9 jit_solution(9803765971716965585)
XLA Ops:
  0.6 91.7 %layer.1 = (bf16[128,2048]{1,0:T(8,128)(2,1)S(1)}, bf16[128,2048]{1,0:T(8,128)(2,1)S(1)}) custom-call(bf16[192,512]{1,0:T(8,128)(2,1)} %bitcast.11, bf16[512,128]{1,0:T(8,128)(2,1)} %bitcast.12, bf16[1,512]{1,0:T(2,128)(2,1)} %refs_2_.1, bf16[128,2048]{1,0:T(8,128)(2,1)} %refs_3_.1, f32[1,2048]{1,0:T(1,128)} %bitcast.13, s32[4,128]{1,0:T(4,128)} %bitcast.14, ...), custom_call_target="tpu_custom_call" | custom-call | flops 10000000000 | bytes 20000000 | tf_op jit(solution)/shard_map/layer/pallas_call | solution.py:888
  92.3 0.8 copy.18
  93.1 0.8 copy.19

commit v3 on v2

--- a/solution.py
+++ b/solution.py
@@ -210,10 +210,10 @@
 ):
     count = lax.axis_size("ep")
     tokens, width = x_ref.shape
-    columns = piece_columns(width)
-    pieces = len(columns)
-    cut = columns[0].stop
-    items = pieces + 1
+    columns, out_columns = piece_columns(width)
+    pieces, out_pieces = len(columns), len(out_columns)
+    cut, out_cut = columns[0].stop, out_columns[0].stop
+    items, out_items = pieces + 1, out_pieces + 1
     z = lax.axis_index("ep")
     t = lax.axis_index("tp")
     x, c = t // 2, t % 2
@@ -553,13 +553,16 @@
 
         both(body)
 
+    def reach(r, start):
+        return slice(start if r == 2 else 0, width)
+
     def result_copy(r, zz, p):
         if p == 0 and r == 3:
             destination, device = rows_in_s.at[zz, band(1)], sibling
         else:
-            destination, device = rows_in.at[zz, band(r), columns[p]], places[r]
+            destination, device = rows_in.at[zz, band(r), out_columns[p]], places[r]
         return copy(
-            chosen.at[zz, band(r), columns[p]],
+            chosen.at[zz, band(r), out_columns[p]],
             destination,
             xr_send.at[r],
             xr_recv.at[r, p, zz],
@@ -567,85 +570,86 @@
             device,
         )
 
-    def reach(r):
-        return slice(cut if r == 2 else 0, width)
-
     def crossing(p):
         return (1, 3) if p == 0 else (3, 2, 1)
 
-    def send_results(zz):
-        for p in range(pieces):
+    def send_results(zz, some=None):
+        for p in some or range(out_pieces):
             for r in crossing(p):
                 result_copy(r, zz, p).start()
 
     def feed_forward(zz, send):
+        now = (out_pieces if send is True else send) if send else 0
         for r in (1, 2, 3):
-            arrived = chosen.at[zz, band(r), reach(r)]
+            arrived = chosen.at[zz, band(r), reach(r, cut)]
             copy(arrived, arrived, xa_send.at[r], xa_recv.at[r, zz], z, sibling).wait_recv()
         gate = jnp.dot(chosen[zz], gate_v[...], preferred_element_type=F32)
         up = jnp.dot(chosen[zz], up_v[...], preferred_element_type=F32)
         hidden = (gate / (1.0 + jnp.exp(-gate)) * up).astype(BF16)
-        for p in range(pieces):
-            rows = jnp.dot(hidden, down_v[:, columns[p]], preferred_element_type=F32).astype(BF16)
-            chosen[zz, :, columns[p]] = rows
-            rows_in[zz, band(0), columns[p]] = rows[band(0)]
+        for p in range(out_pieces):
+            rows = jnp.dot(hidden, down_v[:, out_columns[p]], preferred_element_type=F32).astype(BF16)
+            chosen[zz, :, out_columns[p]] = rows
+            rows_in[zz, band(0), out_columns[p]] = rows[band(0)]
             if p == 0:
                 rows_in_s[zz, band(0)] = rows[band(2)]
 
 
-            if send:
+            if p < now:
                 for r in crossing(p):
                     result_copy(r, zz, p).start()
 
-    def feed_forward_at(distance):
+    def planes_at(distance, act):
         def body(i):
             zz = z - (2 * i - 1) * distance
 
             @pl.when(inside(zz))
             def _():
-                feed_forward(zz, True)
+                act(zz)
 
         both(body)
 
+    def feed_forward_at(distance, send=True):
+        planes_at(distance, lambda zz: feed_forward(zz, send))
+
     def back(i, target, item):
-        if item == pieces:
+        if item == out_pieces:
             source, destination = sums_s.at[target], line_in_s.at[i, target]
         else:
-            source = sums.at[target, :, columns[item]]
-            destination = line_in.at[i, target, :, columns[item]]
+            source = sums.at[target, :, out_columns[item]]
+            destination = line_in.at[i, target, :, out_columns[item]]
         return copy(
             source,
             destination,
-            rz_send.at[1 if item == pieces else 0, target],
+            rz_send.at[1 if item == out_pieces else 0, target],
             rz_recv.at[i, item, target],
             z + 2 * i - 1,
             t,
         )
 
     def total_of(zz, item):
-        if item == pieces:
+        if item == out_pieces:
             result_copy(3, zz, 0).wait_recv()
             acc_s[...] = spread(spreader(1, zz, (0, 1)), rows_in_s[zz])
         elif item == 0:
             result_copy(1, zz, 0).wait_recv()
-            acc[:, columns[0]] = spread(
-                spreader(0, zz, (0, 1)), rows_in[zz, : 2 * capacity, columns[0]]
+            acc[:, out_columns[0]] = spread(
+                spreader(0, zz, (0, 1)), rows_in[zz, : 2 * capacity, out_columns[0]]
             )
         else:
             for r in crossing(item):
                 result_copy(r, zz, item).wait_recv()
-            acc[:, columns[item]] = spread(
-                spreader(0, zz, (0, 1, 2, 3)), rows_in[zz, :, columns[item]]
+            acc[:, out_columns[item]] = spread(
+                spreader(0, zz, (0, 1, 2, 3)), rows_in[zz, :, out_columns[item]]
             )
 
     def take_line(i, zz, item):
         back(i, zz, item).wait_recv()
-        if item == pieces:
+        if item == out_pieces:
             acc_s[...] += line_in_s[i, zz].astype(F32)
         else:
-            acc[:, columns[item]] += line_in[i, zz, :, columns[item]].astype(F32)
-
-    item_order = (pieces, *range(pieces))
+            acc[:, out_columns[item]] += line_in[i, zz, :, out_columns[item]].astype(F32)
+
+    item_order = (out_pieces, *range(out_pieces))
 
     near = jnp.where(2 * z < count, 1, 0)
 
@@ -661,20 +665,25 @@
             def _():
                 take_line(i, target, item)
 
-            if item == pieces:
+            if item == out_pieces:
                 sums_s[target] = acc_s[...].astype(BF16)
             else:
-                sums[target, :, columns[item]] = acc[:, columns[item]].astype(BF16)
+                sums[target, :, out_columns[item]] = acc[:, out_columns[item]].astype(BF16)
             back(i, target, item).start()
 
-    def stage(s):
-        for k in range(items + 2):
-            if k < items:
+    def stage(s, aside=None):
+        for k in range(out_items + 2):
+            if k == 2 and aside:
+                aside()
+            if k < out_items:
                 stage_item(s, near, item_order[k])
             if k >= 2:
                 stage_item(s, 1 - near, item_order[k - 2])
 
     attend_own()
+    early = {}
+    for k in range(out_items):
+        early.setdefault(min(k // 2 + 3, items - 1), []).append(k)
     arrive(1, 0)
     arrive(1, 1)
     shared_expert()
@@ -686,10 +695,16 @@
     for distance in range(2, count):
         last = distance == count - 1
         if not last:
-            pl.when(is_end)(lambda: feed_forward_at(distance - 1))
+
+            @pl.when(is_end)
+            def _():
+                if distance == 2:
+                    send_results(z, (0, 1))
+                feed_forward_at(distance - 1)
+
         for item in range(items):
             if last and item == 3:
-                feed_forward_at(distance - 1)
+                feed_forward_at(distance - 1, 3)
 
                 @pl.when(jnp.logical_not(is_end))
                 def _():
@@ -700,9 +715,14 @@
             if last and item == 2:
                 attend_next(False, heads - 1, heads)
             arrive(distance, item)
+            for k in early.get(item, ()) if distance == 2 and not last else ():
+                stage_item(1, near, item_order[k])
         if not last:
             pl.when(jnp.logical_not(is_end))(lambda: feed_forward_at(distance - 1))
-            stage(distance - 1)
+            if distance > 2:
+                stage(distance - 1)
+        elif 3 < out_pieces:
+            planes_at(distance - 1, lambda zz: send_results(zz, tuple(range(3, out_pieces))))
 
     @pl.when(jnp.logical_not(is_end))
     def _():
@@ -710,20 +730,62 @@
         mixer_move().start()
 
     stage(count - 2)
-    feed_forward_at(count - 1)
 
     @pl.when(is_end)
     def _():
-        send_results(z)
-        project()
-        mixer_move().start()
-
-    stage(count - 1)
+        send_results(z, (2, 3))
+
+    feed_forward_at(count - 1)
+
+    @pl.when(is_end)
+    def _():
+        send_results(z, (4, 5, 6))
+
+    def mix_at_end():
+        @pl.when(is_end)
+        def _():
+            project()
+            mixer_move().start()
+
+    stage(count - 1, mix_at_end)
 
     def last_move():
         return copy(sums_s.at[z], from_side, last_send.at[0], last_recv.at[0], z, side)
 
-    for item in item_order:
+    def drain():
+        for step in range(1, count):
+            for sx in range(2):
+                meta_copy(step, sx).wait_send()
+        meta_copy(0, 1).wait_send()
+        s_move().wait_send()
+
+        @pl.when(sends_kv)
+        def _():
+            for which in range(2):
+                kv_move(which).wait_send()
+
+        for k in range(2):
+            mixer_pair(k).wait_send()
+        for r in (1, 2, 3):
+            sent = staged.at[:, band(r - 1), reach(r, cut)]
+            copy(sent, sent, xa_send.at[r], xa_recv.at[r, 0], z, sibling).wait_send()
+
+        @pl.loop(0, count)
+        def _(zz):
+            for small in range(2):
+                sent = (gathered, gathered_s)[small].at[zz]
+                for i in range(2):
+                    up = 2 * i - 1
+
+                    @pl.when((up * (z - zz) >= 0) & inside(z + up))
+                    def _():
+                        copy(
+                            sent, sent, zs_send.at[i, small, zz], zs_recv.at[0, zz], z, sibling
+                        ).wait_send()
+
+    for k, item in enumerate(item_order):
+        if k == out_items // 2:
+            drain()
         total_of(z, item)
 
         def body(i):
@@ -732,71 +794,45 @@
                 take_line(i, z, item)
 
         both(body)
-        if item == pieces:
+        if item == out_pieces:
             sums_s[z] = acc_s[...].astype(BF16)
             last_move().start()
         elif item > 0:
-            expert_ref[:, columns[item]] = (
-                acc[:, columns[item]] + shared[:, columns[item]]
+            expert_ref[:, out_columns[item]] = (
+                acc[:, out_columns[item]] + shared[:, out_columns[item]]
             ).astype(BF16)
-    last_move().wait_recv()
-    expert_ref[:, columns[0]] = (
-        acc[:, columns[0]] + from_side[...].astype(F32) + shared[:, columns[0]]
-    ).astype(BF16)
+
+    for r in (1, 2, 3):
+        sent = chosen.at[:, band(r), reach(r, out_cut)]
+        copy(sent, sent, xr_send.at[r], xa_recv.at[r, 0], z, sibling).wait_send()
+
+    @pl.loop(0, count)
+    def _(zz):
+        @pl.when(zz != z)
+        def _():
+            for small in range(2):
+                sent = (sums, sums_s)[small].at[zz]
+                copy(sent, sent, rz_send.at[small, zz], zs_recv.at[0, zz], z, sibling).wait_send()
 
     mixer_pair(1).wait_recv()
     mixer_move().wait_recv()
     mixer_ref[...] = (
         terms[0].astype(F32) + mixer_in[1].astype(F32) + mixer_side[...].astype(F32)
     ).astype(BF16)
-
-    for step in range(1, count):
-        for sx in range(2):
-            meta_copy(step, sx).wait_send()
-    meta_copy(0, 1).wait_send()
-    s_move().wait_send()
-
-    @pl.when(sends_kv)
-    def _():
-        for which in range(2):
-            kv_move(which).wait_send()
-
-    for k in range(2):
-        mixer_pair(k).wait_send()
+    last_move().wait_recv()
+    expert_ref[:, out_columns[0]] = (
+        acc[:, out_columns[0]] + from_side[...].astype(F32) + shared[:, out_columns[0]]
+    ).astype(BF16)
     mixer_move().wait_send()
     last_move().wait_send()
 
-    for r in (1, 2, 3):
-        for sent, send in (
-            (staged.at[:, band(r - 1), reach(r)], xa_send),
-            (chosen.at[:, band(r), reach(r)], xr_send),
-        ):
-            copy(sent, sent, send.at[r], xa_recv.at[r, 0], z, sibling).wait_send()
-
-    @pl.loop(0, count)
-    def _(zz):
-        for small in range(2):
-            gather, reduce = ((gathered, sums), (gathered_s, sums_s))[small]
-            for i in range(2):
-                up = 2 * i - 1
-
-                @pl.when((up * (z - zz) >= 0) & inside(z + up))
-                def _():
-                    sent = gather.at[zz]
-                    copy(
-                        sent, sent, zs_send.at[i, small, zz], zs_recv.at[0, zz], z, sibling
-                    ).wait_send()
-
-            @pl.when(zz != z)
-            def _():
-                sent = reduce.at[zz]
-                copy(sent, sent, rz_send.at[small, zz], zs_recv.at[0, zz], z, sibling).wait_send()
-
 
 def piece_columns(width):
     unit = width // 16
-    edges = (0, 2, 5, 8, 10, 12, 14, 16)
-    return [slice(a * unit, b * unit) for a, b in zip(edges, edges[1:])]
+    gather, result = ((0, 2, 5, 8, 10, 12, 14, 16), (0, 3, 5, 8, 10, 12, 14, 16))
+    return tuple(
+        [slice(a * unit, b * unit) for a, b in zip(edges, edges[1:])] for edges in (gather, result)
+    )
 
 
 def layer(
@@ -814,9 +850,9 @@
 ):
     tokens, width = expert_input.shape
     count = lax.axis_size("ep")
-    columns = piece_columns(width)
-    pieces, cut = len(columns), columns[0].stop
-    items = pieces + 1
+    columns, out_columns = piece_columns(width)
+    cut, out_cut = columns[0].stop, out_columns[0].stop
+    items, out_items = len(columns) + 1, len(out_columns) + 1
     span, _, pair_width = key_value.shape
     head_dim = pair_width // 2
     heads = queries.shape[1] // head_dim
@@ -835,14 +871,14 @@
         ((count, capacity, cut), BF16),
         ((count, band, width), BF16),
         ((count, band, width), BF16),
-        ((count, 2 * capacity, cut), BF16),
+        ((count, 2 * capacity, out_cut), BF16),
         ((count, tokens, width), BF16),
-        ((count, tokens, cut), BF16),
+        ((count, tokens, out_cut), BF16),
         ((2, count, tokens, width), BF16),
-        ((2, count, tokens, cut), BF16),
+        ((2, count, tokens, out_cut), BF16),
         ((tokens, width), F32),
-        ((tokens, cut), F32),
-        ((tokens, cut), BF16),
+        ((tokens, out_cut), F32),
+        ((tokens, out_cut), BF16),
         ((tokens, width), F32),
         (out_weight.shape, BF16),
         (shared_parts[0].shape, BF16),
@@ -877,9 +913,9 @@
         (4,),
         (4, count),
         (4,),
-        (4, pieces, count),
+        (4, out_items - 1, count),
         (2, count),
-        (2, items, count),
+        (2, out_items, count),
         (1,),
         (1,),
         (3,),

time: 94 us -> 90.9 us (0.967)
  Pallas kernels: 91.7 us -> 88.5 us
    pallas_call x1, Pallas kernels: 91.7 us -> 88.5 us  [layer(): pl.pallas_call(lambda *refs: layer_kernel(capacity, *refs), out_shape=[pl...]
where the time goes in v3:
time: 90.9 us; the launch traced here: 90.7 us
  Pallas kernels  88.5 us (97%)
  local copies, waits for them, and re-layouts  1.59 us (2%)
    pallas_call x1, Pallas kernels, layer(): pl.pallas_call(lambda *refs: layer_kernel(capacity, *refs), out_shape=[pl...  88.5 us

profile of v3, /device:TPU:0, one launch (start us, length us, event | category | flops | bytes accessed | tf_op | source)
XLA Modules:
  0.0 90.7 jit_solution(14385520801158792098)
XLA Ops:
  0.6 88.5 %layer.1 = (bf16[128,2048]{1,0:T(8,128)(2,1)S(1)}, bf16[128,2048]{1,0:T(8,128)(2,1)S(1)}) custom-call(bf16[192,512]{1,0:T(8,128)(2,1)} %bitcast.11, bf16[512,128]{1,0:T(8,128)(2,1)} %bitcast.12, bf16[1,512]{1,0:T(2,128)(2,1)} %refs_2_.1, bf16[128,2048]{1,0:T(8,128)(2,1)} %refs_3_.1, f32[1,2048]{1,0:T(1,128)} %bitcast.13, s32[4,128]{1,0:T(4,128)} %bitcast.14, ...), custom_call_target="tpu_custom_call" | custom-call | flops 10000000000 | bytes 20000000 | tf_op jit(solution)/shard_map/layer/pallas_call | solution.py:924
  89.1 0.8 copy.18
  89.9 0.8 copy.19

commit v4 on v3

--- a/solution.py
+++ b/solution.py
@@ -671,9 +671,9 @@
                 sums[target, :, out_columns[item]] = acc[:, out_columns[item]].astype(BF16)
             back(i, target, item).start()
 
-    def stage(s, aside=None):
+    def stage(s, aside=None, moment=2):
         for k in range(out_items + 2):
-            if k == 2 and aside:
+            if k == moment and aside:
                 aside()
             if k < out_items:
                 stage_item(s, near, item_order[k])
@@ -704,11 +704,7 @@
 
         for item in range(items):
             if last and item == 3:
-                feed_forward_at(distance - 1, 3)
-
-                @pl.when(jnp.logical_not(is_end))
-                def _():
-                    send_results(z)
+                feed_forward_at(distance - 1, 4)
 
             if distance == 2 and item in (2, 4):
                 attend_next(item == 2, 0 if item == 2 else heads // 2, heads // 2 if item == 2 else heads - 1)
@@ -721,25 +717,20 @@
             pl.when(jnp.logical_not(is_end))(lambda: feed_forward_at(distance - 1))
             if distance > 2:
                 stage(distance - 1)
-        elif 3 < out_pieces:
-            planes_at(distance - 1, lambda zz: send_results(zz, tuple(range(3, out_pieces))))
+        elif 4 < out_pieces:
+            planes_at(distance - 1, lambda zz: send_results(zz, tuple(range(4, out_pieces))))
 
     @pl.when(jnp.logical_not(is_end))
     def _():
+        send_results(z)
         project()
         mixer_move().start()
 
-    stage(count - 2)
+    stage(count - 2, lambda: feed_forward_at(count - 1), 5)
 
     @pl.when(is_end)
     def _():
-        send_results(z, (2, 3))
-
-    feed_forward_at(count - 1)
-
-    @pl.when(is_end)
-    def _():
-        send_results(z, (4, 5, 6))
+        send_results(z, (2, 3, 4, 5, 6))
 
     def mix_at_end():
         @pl.when(is_end)

time: 90.9 us -> 90.9 us (level)
  no operation moved by 1% of the time
where the time goes in v4:
time: 90.9 us; the launch traced here: 90.8 us
  Pallas kernels  88.5 us (97%)
  local copies, waits for them, and re-layouts  1.59 us (2%)
    pallas_call x1, Pallas kernels, layer(): pl.pallas_call(lambda *refs: layer_kernel(capacity, *refs), out_shape=[pl...  88.5 us

profile of v4, /device:TPU:0, one launch (start us, length us, event | category | flops | bytes accessed | tf_op | source)
XLA Modules:
  0.0 90.8 jit_solution(7199846502082235537)
XLA Ops:
  0.6 88.5 %layer.1 = (bf16[128,2048]{1,0:T(8,128)(2,1)S(1)}, bf16[128,2048]{1,0:T(8,128)(2,1)S(1)}) custom-call(bf16[192,512]{1,0:T(8,128)(2,1)} %bitcast.11, bf16[512,128]{1,0:T(8,128)(2,1)} %bitcast.12, bf16[1,512]{1,0:T(2,128)(2,1)} %refs_2_.1, bf16[128,2048]{1,0:T(8,128)(2,1)} %refs_3_.1, f32[1,2048]{1,0:T(1,128)} %bitcast.13, s32[4,128]{1,0:T(4,128)} %bitcast.14, ...), custom_call_target="tpu_custom_call" | custom-call | flops 10000000000 | bytes 20000000 | tf_op jit(solution)/shard_map/layer/pallas_call | solution.py:915
  89.2 0.8 copy.18
  90.0 0.8 copy.19
